TPU v7x, 32 devices: a whole 2x2x4 slice. The times are simulated.
32 devices in a mesh: kv: 16 (over z, y, x), tp: 2 (over core).
Axes of the slice: x: 2, y: 2, z: 4, core: 2. Of those that a mesh axis runs over, the one named last changes fastest.
Arguments:
- tokens: bfloat16 [64, 4, 2048], P('kv', None, 'tp'), may hold values from -6 to 6
- input_gain: float32 [2048], replicated, may hold values from 0.1 to 1.9
- gate_weight: bfloat16 [2048, 4096], P('kv', 'tp'), may hold values from -0.125 to 0.125
- value_weight: bfloat16 [2048, 4096], P('kv', 'tp'), may hold values from -0.125 to 0.125
- write_weight: bfloat16 [2048, 1024], P('kv', 'tp'), may hold values from -0.125 to 0.125
- read_weight: bfloat16 [2048, 1024], P('kv', 'tp'), may hold values from -0.125 to 0.125
- step_weight: bfloat16 [2048, 64], replicated, may hold values from -0.125 to 0.125
- conv_value: float32 [4, 4096], P(None, 'tp'), may hold values from -3 to 3
- conv_write: float32 [4, 1024], P(None, 'tp'), may hold values from -3 to 3
- conv_read: float32 [4, 1024], P(None, 'tp'), may hold values from -3 to 3
- step_bias: float32 [64], P('tp'), may hold values from -4 to -1
- decay_log: float32 [64], P('tp'), may hold values from 0 to 2.8
- skip_gain: float32 [64], P('tp'), may hold values from 0.5 to 1.5
- output_gain: float32 [4096], P('tp'), may hold values from 0.1 to 1.9
- out_weight: bfloat16 [4096, 2048], P('tp', 'kv'), may hold values from -0.09375 to 0.09375
- base_state: float32 [64, 64, 64, 128], P('kv', 'tp'), may hold values from -2 to 2
- past_value: bfloat16 [64, 7, 4096], P('kv', None, 'tp'), may hold values from -6 to 6
- past_write: bfloat16 [64, 7, 1024], P('kv', None, 'tp'), may hold values from -6 to 6
- past_read: bfloat16 [64, 7, 1024], P('kv', None, 'tp'), may hold values from -6 to 6
- past_step: bfloat16 [64, 4, 64], P('kv', None, 'tp'), may hold values from -4 to 4
- accepted: int32 [64], P('kv'), may hold values from 1 to 4
Outputs:
- mixed: bfloat16 [64, 4, 2048], P('kv', None, 'tp')
- root_state: float32 [64, 64, 64, 128], P('kv', 'tp')
- next_value: bfloat16 [64, 7, 4096], P('kv', None, 'tp')
- next_write: bfloat16 [64, 7, 1024], P('kv', None, 'tp')
- next_read: bfloat16 [64, 7, 1024], P('kv', None, 'tp')
- next_step: bfloat16 [64, 4, 64], P('kv', None, 'tp')
Inputs may be any that keep to these rules, and one draw needn't show every extreme that they name: Every entry of `accepted` is an integer from 1 to 4 (at least one of the last step's proposals is always accepted).
All inputs are finite; a program needn't handle non-finite values.
Results may differ from a plain program's by a relative error of at most 0.018.
Values may be sent and summed in bfloat16 or wider, within the bound.
A program may use at most 64 MiB of HBM per device.

v0:
```python
import functools

import jax
import jax.numpy as jnp
from jax import lax
from jax.experimental import pallas as pl
from jax.experimental.pallas import tpu as pltpu
from jax.sharding import PartitionSpec as P

STATE_DIM = 128
CONV_W = 4


EPSILON = 1e-06


def causal_conv(rows, kernel):
    width = kernel.shape[0]
    count = rows.shape[0] - width + 1
    total = kernel[0] * rows[0:count]
    for offset in range(1, width):
        total = total + kernel[offset] * rows[offset : offset + count]
    return total


def advance(
    past_x,
    past_b,
    past_c,
    past_dt,
    taken,
    state_zero,
    value_now,
    write_now,
    read_now,
    gate_now,
    step_now,
    conv_value,
    conv_write,
    conv_read,
    step_bias,
    decay_log,
    skip_gain,
    output_gain,
):
    highest = lax.Precision.DEFAULT
    proposals = value_now.shape[0]
    head_count = step_bias.shape[0]
    group_count = write_now.shape[1] // STATE_DIM
    per_group = head_count // group_count
    head_width = value_now.shape[1] // head_count
    rate = jnp.exp(decay_log)
    prev_x = jax.nn.silu(causal_conv(past_x.astype(jnp.float32), conv_value)).reshape(
        proposals, head_count, head_width
    )
    prev_b = jax.nn.silu(causal_conv(past_b.astype(jnp.float32), conv_write)).reshape(
        proposals, group_count, STATE_DIM
    )
    prev_b = jnp.repeat(prev_b, per_group, axis=1)
    prev_dt = jax.nn.softplus(past_dt.astype(jnp.float32) + step_bias)
    live = (jnp.arange(proposals, dtype=jnp.int32) < taken)[:, None]
    prev_log = jnp.where(live, -rate * prev_dt, jnp.zeros_like(prev_dt))
    total_log = jnp.sum(prev_log, axis=0)
    tail_log = total_log - jnp.cumsum(prev_log, axis=0)
    weight_now = jnp.where(live, jnp.exp(tail_log) * prev_dt, jnp.zeros_like(prev_dt))
    root = jnp.exp(total_log)[:, None, None] * state_zero + jnp.einsum(
        "sh,shp,shn->hpn", weight_now, prev_x, prev_b, precision=highest
    )
    window_x = jnp.concatenate(
        [lax.dynamic_slice_in_dim(past_x, taken, CONV_W - 1, 0), value_now], axis=0
    )
    window_b = jnp.concatenate(
        [lax.dynamic_slice_in_dim(past_b, taken, CONV_W - 1, 0), write_now], axis=0
    )
    window_c = jnp.concatenate(
        [lax.dynamic_slice_in_dim(past_c, taken, CONV_W - 1, 0), read_now], axis=0
    )
    cur_x = jax.nn.silu(causal_conv(window_x.astype(jnp.float32), conv_value)).reshape(
        proposals, head_count, head_width
    )
    cur_b = jax.nn.silu(causal_conv(window_b.astype(jnp.float32), conv_write)).reshape(
        proposals, group_count, STATE_DIM
    )
    cur_c = jax.nn.silu(causal_conv(window_c.astype(jnp.float32), conv_read)).reshape(
        proposals, group_count, STATE_DIM
    )
    cur_b = jnp.repeat(cur_b, per_group, axis=1)
    cur_c = jnp.repeat(cur_c, per_group, axis=1)
    cur_dt = jax.nn.softplus(step_now.astype(jnp.float32) + step_bias)
    logs = jnp.cumsum(-rate * cur_dt, axis=0)
    carried = jnp.einsum("thn,hpn->thp", cur_c, root, precision=highest) * jnp.exp(logs)[:, :, None]
    lower = (jnp.arange(proposals)[:, None] >= jnp.arange(proposals)[None, :])[:, :, None]
    diff = logs[:, None, :] - logs[None, :, :]
    decay = jnp.where(
        lower, jnp.exp(jnp.where(lower, diff, jnp.zeros_like(diff))), jnp.zeros_like(diff)
    )
    scores = (
        jnp.einsum("thn,shn->tsh", cur_c, cur_b, precision=highest) * decay * cur_dt[None, :, :]
    )
    inner = jnp.einsum("tsh,shp->thp", scores, cur_x, precision=highest)
    mixed = carried + inner + skip_gain[None, :, None] * cur_x
    gated = mixed.reshape(proposals, -1) * jax.nn.silu(gate_now.astype(jnp.float32))
    grouped = gated.reshape(proposals, group_count, -1)
    grouped = grouped * lax.rsqrt(jnp.mean(grouped * grouped, axis=-1, keepdims=True) + EPSILON)
    result = (grouped.reshape(proposals, -1) * output_gain).astype(jnp.bfloat16)
    return (result, root, window_x, window_b, window_c)


MESH = pl.DeviceIdType.MESH


def near_split(count):
    low = max(d for d in range(1, count + 1) if count % d == 0 and d * d <= count)
    return count // low, low


def remote(src, dst, send, recv, kv, tp):
    return pltpu.make_async_remote_copy(
        src_ref=src,
        dst_ref=dst,
        send_sem=send,
        recv_sem=recv,
        device_id={"kv": kv, "tp": tp},
        device_id_type=MESH,
    )


class Gather:
    def __init__(self, own, slots, send, recv, n_kv):
        self.own, self.slots, self.send, self.recv = own, slots, send, recv
        self.far, self.near = near_split(n_kv)
        self.me, self.tp = lax.axis_index("kv"), lax.axis_index("tp")
        self.h, self.l = lax.div(self.me, self.near), lax.rem(self.me, self.near)
        self.copies = []

    def start(self, src, block, kv):
        copy = remote(
            src,
            self.slots.at[block],
            self.send.at[len(self.copies)],
            self.recv.at[block],
            kv,
            self.tp,
        )
        copy.start()
        self.copies.append(copy)

    def arrive(self, block):
        remote(
            self.own, self.slots.at[block], self.send.at[0], self.recv.at[block], self.me, self.tp
        ).wait_recv()

    def first(self):
        for step in range(1, self.far):
            self.start(self.own, self.me, lax.rem(self.h + step, self.far) * self.near + self.l)
        for step in range(1, self.near):
            self.start(self.own, self.me, self.h * self.near + lax.rem(self.l + step, self.near))

    def relay(self):
        for step in range(1, self.far):
            block = lax.rem(self.h + self.far - step, self.far) * self.near + self.l
            self.arrive(block)
            for side in range(1, self.near):
                self.start(
                    self.slots.at[block],
                    block,
                    self.h * self.near + lax.rem(self.l + side, self.near),
                )

    def finish(self):
        for side in range(1, self.near):
            l = lax.rem(self.l + self.near - side, self.near)
            for step in range(self.far):
                self.arrive(lax.rem(self.h + self.far - step, self.far) * self.near + l)

    def drain(self):
        for copy in self.copies:
            copy.wait_send()


def project_kernel(
    n_kv, n_tp, x_ref, wide_ref, thin_ref, out_ref,
    xs, wides, thins, mine, back,
    x_send, x_recv, tp_send, tp_recv, wide_send, wide_recv, thin_send, thin_recv,
    back_send, back_recv, local_sem,
):
    me, tp = lax.axis_index("kv"), lax.axis_index("tp")
    barrier = pltpu.get_barrier_semaphore()
    for step in range(1, n_kv):
        pl.semaphore_signal(
            barrier, inc=1, device_id={"kv": lax.rem(me + step, n_kv), "tp": tp}, device_id_type=MESH
        )
    for step in range(1, n_tp):
        pl.semaphore_signal(
            barrier, inc=1, device_id={"kv": me, "tp": lax.rem(tp + step, n_tp)}, device_id_type=MESH
        )
    own = [
        pltpu.make_async_copy(x_ref, xs.at[tp, me], local_sem.at[0]),
        pltpu.make_async_copy(wide_ref.at[me], wides.at[me], local_sem.at[1]),
        pltpu.make_async_copy(thin_ref.at[me], thins.at[me], local_sem.at[2]),
    ]
    for copy in own:
        copy.start()
    pl.semaphore_wait(barrier, n_kv - 1 + n_tp - 1)

    gather = Gather(x_ref, xs.at[tp], x_send, x_recv, n_kv)
    gather.first()
    sends = []

    def send_weights(lo, hi):
        for step in range(lo, hi):
            peer = lax.rem(me + step, n_kv)
            for src, dst, ss, rs in (
                (wide_ref, wides, wide_send, wide_recv),
                (thin_ref, thins, thin_send, thin_recv),
            ):
                copy = remote(src.at[peer], dst.at[me], ss.at[step - 1], rs.at[step - 1], peer, tp)
                copy.start()
                sends.append(copy)

    cut = 1 + n_kv // 4
    send_weights(1, cut)
    gather.relay()
    send_weights(cut, n_kv)
    gather.finish()
    for copy in own:
        copy.wait()
    shares = []
    for step in range(1, n_tp):
        copy = remote(
            xs.at[tp], xs.at[tp], tp_send.at[step - 1], tp_recv.at[step - 1],
            me, lax.rem(tp + step, n_tp),
        )
        copy.start()
        shares.append(copy)
    for copy in shares:
        copy.wait_recv()
    for copy in sends:
        copy.wait_recv()

    tokens = x_ref.shape[0]
    half = x_ref.shape[1]
    depth = wide_ref.shape[1]
    per = n_kv // n_tp
    wide_sum = None
    thin_sum = None
    for t in range(n_tp):
        rows = xs[t].reshape(n_kv * tokens, half)
        block = wides[t * per : (t + 1) * per].reshape(half, wide_ref.shape[2])
        term = jnp.dot(rows, block, preferred_element_type=jnp.float32)
        wide_sum = term if wide_sum is None else wide_sum + term
        for k in range(per):
            term = lax.dot_general(
                rows[:, k * depth : (k + 1) * depth],
                thins[t * per + k],
                (((1,), (1,)), ((), ())),
                preferred_element_type=jnp.float32,
            )
            thin_sum = term if thin_sum is None else thin_sum + term
    wide_cols = wide_ref.shape[2]
    cols = mine.shape[2]
    mine[:, :, 0:wide_cols] = wide_sum.astype(jnp.bfloat16).reshape(n_kv, tokens, wide_cols)
    mine[:, :, wide_cols:cols] = thin_sum.astype(jnp.bfloat16).reshape(
        n_kv, tokens, cols - wide_cols
    )
    returns = []
    for step in range(1, n_kv):
        peer = lax.rem(me + step, n_kv)
        copy = remote(
            mine.at[peer], back.at[me], back_send.at[step - 1], back_recv.at[step - 1], peer, tp
        )
        copy.start()
        returns.append(copy)
    out_ref[me] = mine[me]
    gather.drain()
    for copy in shares + sends:
        copy.wait_send()
    for step, copy in enumerate(returns, 1):
        copy.wait_recv()
        source = lax.rem(me + n_kv - step, n_kv)
        out_ref[source] = back[source]
    for copy in returns:
        copy.wait_send()


def project(x, wide, thin, n_kv, n_tp):
    tokens, half = x.shape
    cols = wide.shape[2] + thin.shape[1]
    dma = pltpu.SemaphoreType.DMA
    far, near = near_split(n_kv)
    count = far - 1 + (near - 1) * far
    peers = (max(n_kv - 1, 1),)
    return pl.pallas_call(
        functools.partial(project_kernel, n_kv, n_tp),
        out_shape=jax.ShapeDtypeStruct((n_kv, tokens, cols), jnp.bfloat16),
        in_specs=[pl.BlockSpec(memory_space=pltpu.VMEM)] * 3,
        out_specs=pl.BlockSpec(memory_space=pltpu.VMEM),
        scratch_shapes=[
            pltpu.VMEM((n_tp, n_kv, tokens, half), jnp.bfloat16),
            pltpu.VMEM(wide.shape, jnp.bfloat16),
            pltpu.VMEM(thin.shape, jnp.bfloat16),
            pltpu.VMEM((n_kv, tokens, cols), jnp.bfloat16),
            pltpu.VMEM((n_kv, tokens, cols), jnp.bfloat16),
            dma((count,)), dma((n_kv,)), dma((max(n_tp - 1, 1),)), dma((max(n_tp - 1, 1),)),
            dma(peers), dma(peers), dma(peers), dma(peers), dma(peers), dma(peers), dma((3,)),
        ],
        compiler_params=pltpu.CompilerParams(collective_id=0, has_side_effects=True),
        name="project",
    )(x, wide, thin)


def mix_kernel(
    n_kv, n_tp, y_ref, w_ref, out_ref,
    ys, mine, parts, y_send, y_recv, part_send, part_recv, local_sem,
):
    me, tp = lax.axis_index("kv"), lax.axis_index("tp")
    total = n_kv * n_tp
    flat = me * n_tp + tp
    barrier = pltpu.get_barrier_semaphore()

    def greet(step, carry):
        other = lax.rem(flat + step, total)
        pl.semaphore_signal(
            barrier,
            inc=1,
            device_id={"kv": lax.div(other, n_tp), "tp": lax.rem(other, n_tp)},
            device_id_type=MESH,
        )
        return carry

    lax.fori_loop(1, total, greet, 0)
    own = pltpu.make_async_copy(y_ref, ys.at[me], local_sem.at[0])
    own.start()
    pl.semaphore_wait(barrier, total - 1)
    gather = Gather(y_ref, ys, y_send, y_recv, n_kv)
    gather.first()
    gather.relay()
    own.wait()
    gather.finish()

    tokens, cols = y_ref.shape[0], w_ref.shape[1]
    product = jnp.dot(
        ys[...].reshape(n_kv * tokens, y_ref.shape[1]),
        w_ref[...],
        preferred_element_type=jnp.float32,
    )
    mine[...] = product.astype(jnp.bfloat16).reshape(n_kv, tokens, cols)
    per = n_kv // n_tp
    side, place = lax.div(me, per), lax.rem(me, per)

    def part(step):
        return remote(
            mine.at[lax.rem(me + step, n_kv)],
            parts.at[tp, place],
            part_send.at[step],
            part_recv.at[tp, place],
            lax.rem(me + step, n_kv),
            side,
        )

    for step in range(1, n_kv):
        part(step).start()

    @pl.when(side != tp)
    def _():
        part(0).start()

    @pl.when(side == tp)
    def _():
        parts[tp, place] = mine[me]

    gather.drain()
    for t in range(n_tp):
        for k in range(per):
            incoming = remote(
                mine.at[0], parts.at[t, k], part_send.at[0], part_recv.at[t, k], me, tp
            )

            @pl.when(jnp.logical_or(t != tp, tp * per + k != me))
            def _():
                incoming.wait_recv()

    for k in range(per):
        value = parts[0, k].astype(jnp.float32)
        for t in range(1, n_tp):
            value = value + parts[t, k].astype(jnp.float32)
        out_ref[:, k * cols : (k + 1) * cols] = value.astype(jnp.bfloat16)
    for step in range(1, n_kv):
        part(step).wait_send()

    @pl.when(side != tp)
    def _():
        part(0).wait_send()


def mix(y, weight, n_kv, n_tp):
    tokens, depth = y.shape
    cols = weight.shape[1]
    dma = pltpu.SemaphoreType.DMA
    far, near = near_split(n_kv)
    count = far - 1 + (near - 1) * far
    per = n_kv // n_tp
    return pl.pallas_call(
        functools.partial(mix_kernel, n_kv, n_tp),
        out_shape=jax.ShapeDtypeStruct((tokens, per * cols), jnp.bfloat16),
        in_specs=[pl.BlockSpec(memory_space=pltpu.VMEM)] * 2,
        out_specs=pl.BlockSpec(memory_space=pltpu.VMEM),
        scratch_shapes=[
            pltpu.VMEM((n_kv, tokens, depth), jnp.bfloat16),
            pltpu.VMEM((n_kv, tokens, cols), jnp.bfloat16),
            pltpu.VMEM((n_tp, per, tokens, cols), jnp.bfloat16),
            dma((count,)), dma((n_kv,)), dma((n_kv,)), dma((n_tp, per)), dma((1,)),
        ],
        compiler_params=pltpu.CompilerParams(collective_id=1, has_side_effects=True),
        name="mix",
    )(y, weight)


def on_device(
    tokens,
    input_gain,
    gate_weight,
    value_weight,
    write_weight,
    read_weight,
    step_weight,
    conv_value,
    conv_write,
    conv_read,
    step_bias,
    decay_log,
    skip_gain,
    output_gain,
    out_weight,
    base_state,
    past_value,
    past_write,
    past_read,
    past_step,
    accepted,
):
    whole = lax.all_gather(tokens, "tp", axis=2, tiled=True)
    seq_local, proposals, width = whole.shape
    rows = whole.astype(jnp.float32)
    normed = (
        rows * lax.rsqrt(jnp.mean(rows * rows, axis=-1, keepdims=True) + EPSILON) * input_gain
    ).astype(jnp.bfloat16)
    flat = normed.reshape(seq_local * proposals, width)
    token_count = flat.shape[0]
    head_count = step_bias.shape[0]
    own_step = lax.dynamic_slice_in_dim(
        step_weight, lax.axis_index("tp") * head_count, head_count, 1
    )
    step_now = jnp.dot(flat, own_step, preferred_element_type=jnp.float32).astype(jnp.bfloat16)
    ranks, n_tp = lax.axis_size("kv"), lax.axis_size("tp")
    depth = gate_weight.shape[0]
    cut = [
        item.reshape(depth, ranks, item.shape[1] // ranks)
        for item in (gate_weight, value_weight, write_weight, read_weight)
    ]
    spans = [item.shape[2] for item in cut]
    wide = jnp.concatenate(cut[:2], axis=2).transpose(1, 0, 2)
    thin = jnp.concatenate(cut[2:], axis=2).transpose(1, 2, 0)
    half = width // n_tp
    own_features = lax.dynamic_slice_in_dim(flat, lax.axis_index("tp") * half, half, 1)
    returned = project(own_features, wide, thin, ranks, n_tp).transpose(1, 0, 2)
    pieces_out = []
    offset = 0
    for span in spans:
        pieces_out.append(returned[:, :, offset : offset + span].reshape(token_count, ranks * span))
        offset = offset + span
    gate_now, value_now, write_now, read_now = pieces_out
    shaped = [
        item.reshape(seq_local, proposals, item.shape[1])
        for item in (value_now, write_now, read_now, gate_now, step_now)
    ]
    stepper = jax.vmap(advance, in_axes=(0,) * 11 + (None,) * 7)
    normal_out, root_state, next_value, next_write, next_read = stepper(
        past_value,
        past_write,
        past_read,
        past_step,
        accepted,
        base_state,
        shaped[0],
        shaped[1],
        shaped[2],
        shaped[3],
        shaped[4],
        conv_value,
        conv_write,
        conv_read,
        step_bias,
        decay_log,
        skip_gain,
        output_gain,
    )
    flat_y = normal_out.reshape(token_count, -1)
    mixed = mix(flat_y, out_weight, ranks, n_tp)
    mixed = mixed.reshape(seq_local, proposals, mixed.shape[1])
    return (mixed, root_state, next_value, next_write, next_read, shaped[4])


def solution(mesh):
    return jax.shard_map(
        on_device,
        mesh=mesh,
        in_specs=(
            P("kv", None, "tp"),
            P(),
            P("kv", "tp"),
            P("kv", "tp"),
            P("kv", "tp"),
            P("kv", "tp"),
            P(),
            P(None, "tp"),
            P(None, "tp"),
            P(None, "tp"),
            P("tp"),
            P("tp"),
            P("tp"),
            P("tp"),
            P("tp", "kv"),
            P("kv", "tp", None, None),
            P("kv", None, "tp"),
            P("kv", None, "tp"),
            P("kv", None, "tp"),
            P("kv", None, "tp"),
            P("kv"),
        ),
        out_specs=(
            P("kv", None, "tp"),
            P("kv", "tp", None, None),
            P("kv", None, "tp"),
            P("kv", None, "tp"),
            P("kv", None, "tp"),
            P("kv", None, "tp"),
        ),
        check_vma=False,
    )
```

profile of v0, /device:TPU:0, one launch (start us, length us, event | category | flops | bytes accessed | tf_op | source)
XLA Modules:
  0.0 108.6 jit_solution(16907155390508896206)
XLA Ops:
  0.6 0.0 copy-start
  0.7 2.3 %all_gather.3 = bf16[4,4,2048]{2,1,0:T(4,128)(2,1)S(1)} all-gather(bf16[4,4,1024]{2,1,0:T(4,128)(2,1)} %param.21), channel_id=1, replica_groups=mesh['kv'=16,'tp'=2] {'tp'}, dimensions={2}, use_global_device_ids=true | all-gather | bytes 98304 | tf_op jit(solution)/shard_map/all_gather | solution.py:442
  3.0 0.1 fusion.9
  3.1 0.8 fusion.11
  4.0 0.6 constant_dynamic-slice_fusion.x_ref
  4.6 1.3 %copy.146 = bf16[128,2048]{0,1:T(8,128)(2,1)S(1)} copy(bf16[128,2048]{1,0:T(8,128)(2,1)} %param.23) | data formatting | bytes 1048576 | tf_op args[2]
  5.9 0.0 copy-start.15
  5.9 0.0 copy-start.1
  5.9 0.3 copy.148
  6.2 1.3 %copy.147 = bf16[128,2048]{0,1:T(8,128)(2,1)S(1)} copy(bf16[128,2048]{1,0:T(8,128)(2,1)} %param.24) | data formatting | bytes 1048576 | tf_op args[3]
  7.6 0.0 copy-start.7
  7.6 0.3 copy.149
  7.9 0.0 copy-start.3
  7.9 1.1 %maximum_bitcast_fusion.wide_ref = bf16[16,128,256]{2,1,0:T(8,128)(2,1)} fusion(bf16[128,16,128]{2,0,1:T(8,128)(2,1)S(1)} %copy.149, bf16[128,16,128]{2,0,1:T(8,128)(2,1)S(1)} %copy.148), kind=kLoop, calls=%fused_computation.9 | loop fusion | flops 2097152 | bytes 2097152 | tf_op jit(solution)/shard_map/transpose | solution.py:462
  9.0 0.0 copy-start.13
  9.0 0.1 copy.150
  9.2 0.1 copy.151
  9.3 0.7 maximum_bitcast_fusion.1.thin_ref
  10.0 55.0 %project.1 = bf16[16,16,320]{2,1,0:T(8,128)(2,1)} custom-call(bf16[16,1024]{1,0:T(8,128)(2,1)} %constant_dynamic-slice_fusion.x_ref, bf16[16,128,256]{2,1,0:T(8,128)(2,1)} %maximum_bitcast_fusion.wide_ref, bf16[16,64,128]{2,1,0:T(8,128)(2,1)} %maximum_bitcast_fusion.1.thin_ref), custom_call_target="tpu_custom_call" | custom-call | tf_op jit(solution)/shard_map/project/pallas_call | solution.py:293
  65.0 0.0 copy-start.2
  65.0 0.9 fusion.44
  66.0 0.8 gather_fusion.1
  66.9 0.1 pad_maximum_fusion
  67.1 0.3 divide_multiply_fusion.1
  67.4 0.2 reshape.154
  67.6 0.0 copy-done.2
  67.6 0.1 fusion.57
  67.7 0.1 reshape_reshape.12
  67.8 0.0 copy-done.3
  67.8 0.6 gather_fusion.2
  68.5 0.1 fusion.43
  68.7 0.0 copy-done
  68.7 0.1 convolution_convert_fusion
  68.9 0.1 iota_compare_fusion.1
  69.0 0.1 fusion.56
  69.1 0.1 multiply_select_fusion
  69.2 0.1 copy.141
  69.3 0.0 copy-start.4
  69.3 0.0 copy-start.12
  69.3 5.8 %multiply_add_fusion = f32[4,32,64,128]{3,2,1,0:T(8,128)} fusion(f32[4,32,64,128]{3,2,1,0:T(8,128)} %param.36, bf16[4,4,32,128]{3,1,2,0:T(4,128)(2,1)S(1)} %bitcast.95, f32[4,32]{1,0:T(4,128)S(1)} %exp.62, f32[4,4,32,64]{3,2,1,0:T(8,128)S(1)} %reshape.154, f32[4,4,32]{1,2,0:T(8,128)S(1)} %copy.141), kind=kOutput, calls=%fused_computation.3 | convolution fusion | flops 10518528 | bytes 8653312 | tf_op jit(solution)/shard_map/vmap(sh,shp,shn->hpn)/dot_general | solution.py:66
  75.1 0.0 copy-done.8
  75.1 0.1 reshape_reshape.10
  75.2 0.6 gather_fusion
  76.0 0.1 fusion.42
  76.0 0.0 copy-start.14
  76.1 0.0 copy-start.10
  76.1 3.4 %fusion.61 = f32[4,32,64,4]{2,3,1,0:T(4,128)S(1)} fusion(f32[4,32,64,128]{3,2,1,0:T(8,128)} %multiply_add_fusion, bf16[4,4,32,128]{3,1,2,0:T(4,128)(2,1)S(1)} %bitcast.96), kind=kOutput, calls=%fused_computation.120 | convolution fusion | flops 8388608 | bytes 4456448 | tf_op jit(solution)/shard_map/vmap(thn,hpn->thp)/dot_general | solution.py:91
  79.5 0.2 reshape.165
  79.8 0.1 copy.161
  79.9 0.1 copy.163
  80.0 0.8 fusion.2
  80.9 0.1 reshape.171
  81.0 0.3 multiply_reduce_fusion
  81.3 0.1 copy.175
  81.4 0.1 copy.170
  81.5 0.1 mul.379
  81.7 0.1 reshape.168
  81.8 0.0 copy-done.10
  81.8 0.7 fusion.30.y_ref
  82.5 22.7 %mix.1 = bf16[16,1024]{1,0:T(8,128)(2,1)} custom-call(bf16[16,2048]{1,0:T(8,128)(2,1)} %fusion.30.y_ref, bf16[2048,128]{1,0:T(8,128)(2,1)} %w_ref.1), custom_call_target="tpu_custom_call" | custom-call | tf_op jit(solution)/shard_map/mix/pallas_call | solution.py:403
  105.2 1.4 %reshape.169 = bf16[4,4,1024]{2,1,0:T(4,128)(2,1)} reshape(bf16[16,1024]{1,0:T(8,128)(2,1)} %mix.1) | data formatting | bytes 65536 | tf_op jit(solution)/shard_map/reshape | solution.py:500
  106.6 0.7 copy.171
  107.3 0.6 copy.172
  108.0 0.6 copy.173
  (46 shorter events, 0.7 us)
Async XLA Ops:
  0.6 68.1 %copy-start = (bf16[2048,64]{0,1:T(8,128)(2,1)S(1)}, bf16[2048,64]{0,1:T(8,128)(2,1)}, u32[]{:S(2)}) copy-start(bf16[2048,64]{0,1:T(8,128)(2,1)} %param.27) | copy-start | bytes 786436
  0.6 8.4 %copy-start.5 = (bf16[128,512]{1,0:T(8,128)(2,1)S(1)}, bf16[128,512]{1,0:T(8,128)(2,1)}, u32[]{:S(2)}) copy-start(bf16[128,512]{1,0:T(8,128)(2,1)} %param.25) | copy-start | bytes 393220
  0.7 8.5 %copy-start.6 = (bf16[128,512]{1,0:T(8,128)(2,1)S(1)}, bf16[128,512]{1,0:T(8,128)(2,1)}, u32[]{:S(2)}) copy-start(bf16[128,512]{1,0:T(8,128)(2,1)} %param.26) | copy-start | bytes 393220
  5.9 60.1 %copy-start.15 = (s32[4]{0:T(128)S(1)}, s32[4]{0:T(128)}, u32[]{:S(2)}) copy-start(s32[4]{0:T(128)} %param.41) | copy-start | bytes 52
  5.9 60.1 %copy-start.1 = (bf16[4,7,2048]{2,0,1:T(4,128)(2,1)S(1)}, bf16[4,7,2048]{2,0,1:T(4,128)(2,1)}, u32[]{:S(2)}) copy-start(bf16[4,7,2048]{2,0,1:T(4,128)(2,1)} %param.37) | copy-start | bytes 344068
  7.6 59.5 %copy-start.7 = (f32[4,2048]{1,0:T(4,128)S(1)}, f32[4,2048]{1,0:T(4,128)}, u32[]{:S(2)}) copy-start(f32[4,2048]{1,0:T(4,128)} %param.28) | copy-start | bytes 98308
  7.9 60.0 %copy-start.3 = (bf16[4,7,512]{2,0,1:T(4,128)(2,1)S(1)}, bf16[4,7,512]{2,0,1:T(4,128)(2,1)}, u32[]{:S(2)}) copy-start(bf16[4,7,512]{2,0,1:T(4,128)(2,1)} %param.38) | copy-start | bytes 86020
  9.0 59.5 %copy-start.11 = (f32[4,512]{1,0:T(4,128)S(1)}, f32[4,512]{1,0:T(4,128)}, u32[]{:S(2)}) copy-start(f32[4,512]{1,0:T(4,128)} %param.29) | copy-start | bytes 24580
  9.0 59.9 %copy-start.16 = (f32[32]{0:T(128)S(1)}, f32[32]{0:T(128)}, u32[]{:S(2)}) copy-start(f32[32]{0:T(128)} %param.32) | copy-start | bytes 388
  9.0 60.0 %copy-start.9 = (bf16[4,4,32]{2,1,0:T(4,128)(2,1)S(1)}, bf16[4,4,32]{2,1,0:T(4,128)(2,1)}, u32[]{:S(2)}) copy-start(bf16[4,4,32]{2,1,0:T(4,128)(2,1)} %param.40) | copy-start | bytes 3076
  9.0 60.0 %copy-start.13 = (f32[32]{0:T(128)S(1)}, f32[32]{0:T(128)}, u32[]{:S(2)}) copy-start(f32[32]{0:T(128)} %param.31) | copy-start | bytes 388
  65.0 2.6 %copy-start.2 = (bf16[16,16,320]{2,1,0:T(8,128)(2,1)S(1)}, bf16[16,16,320]{2,1,0:T(8,128)(2,1)}, u32[]{:S(2)}) copy-start(bf16[16,16,320]{2,1,0:T(8,128)(2,1)} %project.1) | copy-start | bytes 491524
  68.9 6.2 %copy-start.8 = (bf16[16,32]{1,0:T(8,128)(2,1)}, bf16[16,32]{1,0:T(8,128)(2,1)S(1)}, u32[]{:S(2)}) copy-start(bf16[16,32]{1,0:T(8,128)(2,1)S(1)} %convolution_convert_fusion) | copy-start | bytes 3076
  69.3 5.9 %copy-start.4 = (bf16[4,7,512]{2,0,1:T(4,128)(2,1)S(1)}, bf16[4,7,512]{2,0,1:T(4,128)(2,1)}, u32[]{:S(2)}) copy-start(bf16[4,7,512]{2,0,1:T(4,128)(2,1)} %param.39) | copy-start | bytes 86020
  69.3 6.6 %copy-start.12 = (f32[4,512]{1,0:T(4,128)S(1)}, f32[4,512]{1,0:T(4,128)}, u32[]{:S(2)}) copy-start(f32[4,512]{1,0:T(4,128)} %param.30) | copy-start | bytes 24580
  76.0 4.9 %copy-start.14 = (f32[32]{0:T(128)S(1)}, f32[32]{0:T(128)}, u32[]{:S(2)}) copy-start(f32[32]{0:T(128)} %param.33) | copy-start | bytes 388
  76.1 5.7 %copy-start.10 = (f32[2048]{0:T(1024)S(1)}, f32[2048]{0:T(1024)}, u32[]{:S(2)}) copy-start(f32[2048]{0:T(1024)} %param.34) | copy-start | bytes 24580
where the time goes:
time: 109 us
  Pallas kernels  77.7 us (71%)
  local copies, waits for them, and re-layouts  11.6 us (11%)
  matrix products  10.1 us (9%)
  other arithmetic  5.76 us (5%)
  blocking collectives  2.34 us (2%)
  between operations  1.13 us (1%)
    pallas_call x1, Pallas kernels, project(): pl.pallas_call(functools.partial(project_kernel, n_kv, n_tp), out_shape=j...  55 us
    pallas_call x1, Pallas kernels, mix(): pl.pallas_call(functools.partial(mix_kernel, n_kv, n_tp), out_shape=jax.S...  22.7 us
    dot_general x1, matrix products, advance(): jnp.einsum('sh,shp,shn->hpn', weight_now, prev_x, prev_b, precision=highest)  5.77 us
    unnamed x43, local copies, waits for them, and re-layouts  5.09 us
    dot_general x1, matrix products, advance(): jnp.einsum('thn,hpn->thp', cur_c, root, precision=highest)  3.37 us
    all_gather x1, blocking collectives, on_device(): whole = lax.all_gather(tokens, 'tp', axis=2, tiled=True)  2.34 us

commit v1 on v0

v1 whole, which is shorter than its diff:
```python
import functools
from typing import NamedTuple

import jax
import jax.numpy as jnp
from jax import lax
from jax.experimental import pallas as pl
from jax.experimental.pallas import tpu as pltpu
from jax.sharding import PartitionSpec as P

STATE_DIM = 128
LANES = 128
EPSILON = 1e-06
MESH = pl.DeviceIdType.MESH
F32 = jnp.float32
BF16 = jnp.bfloat16


class Dims(NamedTuple):
    far: int
    near: int
    n_tp: int
    seqs: int
    props: int
    taps: int
    width: int
    feats: int
    depth: int
    groups: int
    gw: int
    heads: int
    out_cols: int

    @property
    def rows(self):
        return self.seqs * self.props

    @property
    def n_kv(self):
        return self.far * self.near

    @property
    def block(self):
        return self.near * self.depth

    @property
    def part(self):
        return self.gw // self.near

    @property
    def every(self):
        return self.near // 2

    def thin(self, g):
        return g % self.every == 0

    def cols(self, g):
        return 2 * self.part + (STATE_DIM if self.thin(g) else 0)


def near_size(n_kv, gw):
    return max(
        d
        for d in range(2, n_kv + 1, 2)
        if n_kv % d == 0 and d * d <= n_kv and gw % (LANES * d) == 0
    )


def remote(src, dst, send, recv, kv, tp):
    return pltpu.make_async_remote_copy(
        src_ref=src,
        dst_ref=dst,
        send_sem=send,
        recv_sem=recv,
        device_id={"kv": kv, "tp": tp},
        device_id_type=MESH,
    )


def silu(v):
    return v / (1.0 + jnp.exp(-v))


def softplus(v):
    return jnp.maximum(v, 0.0) + jnp.log1p(jnp.exp(-jnp.abs(v)))


def conv(rows, taps, count):
    out = []
    for t in range(count):
        total = taps[0] * rows[t]
        for k in range(1, len(taps)):
            total = total + taps[k] * rows[t + k]
        out.append(total)
    return out


NT = (((1,), (1,)), ((), ()))


def mixer_kernel(d, *refs):
    (
        tok, gain, gate_w, value_w, write_w, read_w, step_w, conv_v, conv_b, conv_c, head_p,
        wout_h, base_h, past_v, past_b, past_c, past_s, taken_ref,
    ) = refs[:18]
    mixed, root_h, next_v, next_b, next_c, next_s = refs[18:24]
    rest = list(refs[24:])
    G = d.groups
    stage, wbuf, zmine, zin, red, back, rootb, ys = (rest[i * G : (i + 1) * G] for i in range(8))
    (
        xq, xs, pt_mine, pt_in, base_v, wout, acc, mine, parts,
        ssem, w_sem, xz_sem, xp_sem, pt_sem, z_sem, b_sem, y_sem, m_sem, l_sem,
    ) = rest[8 * G :]
    far, near, n_tp, rows, S, N = d.far, d.near, d.n_tp, d.rows, d.seqs, STATE_DIM
    n_kv, part, gw, props = d.n_kv, d.part, d.gw, d.props
    me, tp = lax.axis_index("kv"), lax.axis_index("tp")
    h, l = lax.div(me, near), lax.rem(me, near)

    total = n_kv * n_tp
    flat = me * n_tp + tp
    barrier = pltpu.get_barrier_semaphore()

    def greet(step, carry):
        other = lax.rem(flat + step, total)
        pl.semaphore_signal(
            barrier,
            inc=1,
            device_id={"kv": lax.div(other, n_tp), "tp": lax.rem(other, n_tp)},
            device_id_type=MESH,
        )
        return carry

    lax.fori_loop(1, total, greet, 0)

    used = []

    def local(src, dst):
        copy = pltpu.make_async_copy(src, dst, l_sem.at[len(used)])
        copy.start()
        used.append(copy)
        return copy

    units = 2 * G
    staging = []
    for g in range(G):
        copies = []
        for k in range(near):
            lo = g * gw + k * part
            copies.append(local(gate_w.at[:, lo : lo + part], stage[g].at[k, :, 0:part]))
            copies.append(local(value_w.at[:, lo : lo + part], stage[g].at[k, :, part : 2 * part]))
            if d.thin(g):
                u = (g // d.every * near + k) % units
                source = (write_w, read_w)[u % 2]
                copies.append(
                    local(
                        source.at[:, u // 2 * N : (u // 2 + 1) * N],
                        stage[g].at[k, :, 2 * part : 2 * part + N],
                    )
                )
        staging.append(copies)
    loading = [
        local(base_h.at[:, g * gw : (g + 1) * gw], base_v.at[:, g * gw : (g + 1) * gw])
        for g in range(G)
    ]
    wout_load = local(wout_h, wout)

    sends = []

    def send(src, dst, recv, kv, t, cond=None):
        copy = remote(src, dst, ssem.at[len(sends)], recv, kv, t)
        sends.append((copy, cond))
        if cond is None:
            copy.start()
        else:
            pl.when(cond)(copy.start)

    def arrive(dst, recv, cond=None):
        copy = remote(dst, dst, ssem.at[0], recv, me, tp)
        if cond is None:
            copy.wait_recv()
        else:
            pl.when(cond)(copy.wait_recv)

    nb = d.feats // d.block
    own = pl.multiple_of(tp * d.feats, d.feats)
    raw = tok[...].astype(F32)
    square = jnp.sum(raw * raw, axis=-1, keepdims=True)
    scaled = (raw * gain[:, pl.ds(own, d.feats)]).astype(BF16)
    for q in range(nb):
        xq[q] = scaled[:, q * d.block : (q + 1) * d.block]
    hpad = pt_mine.shape[2] - LANES
    for t in range(n_tp):
        term = lax.dot_general(
            scaled, step_w[t * d.heads : (t + 1) * d.heads, pl.ds(own, d.feats)], NT,
            preferred_element_type=F32,
        )
        pt_mine[t, :, 0 : d.heads] = term
        pt_mine[t, :, hpad : hpad + LANES] = jnp.broadcast_to(square, (rows, LANES))
    pt_in[tp] = pt_mine[tp]

    pl.semaphore_wait(barrier, total - 1)

    home = lax.div(h, nb)
    for q in range(nb):
        plane = tp * nb + q
        for t in range(n_tp):
            away = jnp.logical_or(plane != h, tp != t)
            send(xq.at[q], xs.at[l, h], xz_sem.at[h], plane * near + l, t, away)

    @pl.when(home == tp)
    def _():
        xs[l, h] = xq[lax.rem(h, nb)]

    for step in range(1, n_tp):
        t = lax.rem(tp + step, n_tp)
        send(pt_mine.at[t], pt_in.at[tp], pt_sem.at[tp], me, t)

    def send_weights(g):
        for copy in staging[g]:
            copy.wait()
        for step in range(1, near):
            k = lax.rem(l + step, near)
            send(stage[g].at[k], wbuf[g].at[l], w_sem.at[g, l], h * near + k, tp)

    send_weights(0)

    taken = taken_ref[...]
    row_seq = lax.rem(lax.broadcasted_iota(jnp.int32, (rows, N), 0), S)

    def spread(g):
        r = lax.broadcasted_iota(jnp.int32, (d.heads, gw), 0)
        c = lax.broadcasted_iota(jnp.int32, (d.heads, gw), 1)
        hw = gw * G // d.heads
        lo = r * hw - g * gw
        return jnp.where(jnp.logical_and(c >= lo, c < lo + hw), 1.0, 0.0).astype(BF16)

    def span(g, w):
        return slice(g * w, (g + 1) * w)

    def taps(ref, cols):
        return [ref[k : k + 1, cols] for k in range(d.taps)]

    def param(k, g):
        return head_p[k : k + 1, span(g, gw)]

    def pieces(v):
        return [v[t * S : (t + 1) * S] for t in range(props)]

    def old(ref, cols):
        return [ref[i, :, cols].astype(F32) for i in range(ref.shape[0])]

    def root(g):
        loading[g].wait()
        cv, cn = span(g, gw), span(g, N)
        px = [silu(v) for v in conv(old(past_v, cv), taps(conv_v, cv), props)]
        pb = [silu(v) for v in conv(old(past_b, cn), taps(conv_b, cn), props)]
        pd = softplus(
            jnp.dot(past_s[...], spread(g), preferred_element_type=F32) + param(0, g)
        )
        rate = jnp.exp(param(1, g))
        pd = pieces(pd)
        log = [jnp.where(taken > t, -rate * pd[t], 0.0) for t in range(props)]
        tail = jnp.zeros_like(log[0])
        weighted = [None] * props
        for t in reversed(range(props)):
            weighted[t] = jnp.where(taken > t, jnp.exp(tail) * pd[t], 0.0) * px[t]
            tail = tail + log[t]
        left = jnp.transpose(jnp.concatenate(weighted, axis=0)).astype(BF16)
        decay = jnp.exp(tail)
        fill = [decay] * max(1, 8 // S)
        decay = jnp.transpose(jnp.concatenate(fill, axis=0))
        right = jnp.concatenate(pb, axis=0)
        for s in range(S):
            outer = jnp.dot(
                left,
                jnp.where(row_seq == s, right, 0.0).astype(BF16),
                preferred_element_type=F32,
            )
            new = decay[:, s : s + 1] * base_v[s, cv, :] + outer
            base_v[s, cv, :] = new
            rootb[g][:, span(s, N)] = new.astype(BF16)
        return local(base_v.at[:, cv], root_h.at[:, cv])

    stores = [root(0)]

    for k in range(far):
        arrive(
            xs.at[l, k], xz_sem.at[k], jnp.logical_or(h != k, home != tp)
        )
    for step in range(1, near):
        send(xs.at[l], xs.at[l], xp_sem.at[l], h * near + lax.rem(l + step, near), tp)
    for g in range(1, G):
        send_weights(g)

    for step in range(1, n_tp):
        t = lax.rem(tp + n_tp - step, n_tp)
        arrive(pt_in.at[t], pt_sem.at[t])
    joined = pt_in[0]
    for t in range(1, n_tp):
        joined = joined + pt_in[t]
    scale = lax.rsqrt(joined[:, hpad : hpad + LANES] * (1.0 / d.width) + EPSILON)
    step_now = (joined[:, 0 : d.heads] * scale[:, 0 : d.heads]).astype(BF16)
    next_s[...] = step_now

    for step in range(1, near):
        k = lax.rem(l + near - step, near)
        arrive(xs.at[k], xp_sem.at[k])

    def project(g):
        wbuf[g][l] = stage[g][l]
        for step in range(1, near):
            k = lax.rem(l + near - step, near)
            arrive(wbuf[g].at[k], w_sem.at[g, k])
        cols = d.cols(g)
        product = jnp.dot(
            xs[...].reshape(n_kv * rows, d.block),
            wbuf[g][...].reshape(d.block, cols),
            preferred_element_type=F32,
        ).astype(BF16)
        for k in range(near):
            for z in range(far):
                at = (k * far + z) * rows
                zmine[g][z, k] = product[at : at + rows]
        for step in range(1, far):
            z = lax.rem(h + step, far)
            send(zmine[g].at[z], zin[g].at[h], z_sem.at[g, h], z * near + l, tp)

    def collect(g):
        value = zmine[g][h].astype(F32)
        for step in range(1, far):
            z = lax.rem(h + far - step, far)
            arrive(zin[g].at[z], z_sem.at[g, z])
            value = value + zin[g][z].astype(F32)
        red[g][...] = value.astype(BF16)
        back[g][l] = red[g][l]
        for step in range(1, near):
            k = lax.rem(l + step, near)
            send(red[g].at[k], back[g].at[l], b_sem.at[g, l], h * near + k, tp)

    def rounded(piece):
        return (piece.astype(F32) * scale).astype(BF16).astype(F32)

    def advance(g):
        for step in range(1, near):
            k = lax.rem(l + near - step, near)
            arrive(back[g].at[k], b_sem.at[g, k])
        cv, cn = span(g, gw), span(g, N)
        gate = jnp.concatenate([rounded(back[g][k, :, 0:part]) for k in range(near)], axis=1)
        value = jnp.concatenate(
            [rounded(back[g][k, :, part : 2 * part]) for k in range(near)], axis=1
        )

        def unit(u):
            j, k = u // near, u % near
            return rounded(back[j * d.every][k, :, 2 * part : 2 * part + N])

        def window(past, now, out, cols):
            before = old(past, cols)
            rows_now = []
            for i in range(d.taps - 1):
                row = before[i + 1]
                for a in range(2, props + 1):
                    row = jnp.where(taken == a, before[i + a], row)
                rows_now.append(row)
            rows_now = rows_now + pieces(now)
            for i, row in enumerate(rows_now):
                out[i, :, cols] = row.astype(BF16)
            return rows_now

        win_v = window(past_v, value, next_v, cv)
        win_b = window(past_b, unit(2 * g), next_b, cn)
        win_c = window(past_c, unit(2 * g + 1), next_c, cn)
        x = [silu(v) for v in conv(win_v, taps(conv_v, cv), props)]
        b = [silu(v) for v in conv(win_b, taps(conv_b, cn), props)]
        c = [silu(v) for v in conv(win_c, taps(conv_c, cn), props)]
        whole = jnp.concatenate(c, axis=0)
        masked = jnp.concatenate(
            [jnp.where(row_seq == s, whole, 0.0) for s in range(S)], axis=1
        ).astype(BF16)
        carried = pieces(
            lax.dot_general(masked, rootb[g][...], NT, preferred_element_type=F32)
        )
        dt = pieces(
            softplus(jnp.dot(step_now, spread(g), preferred_element_type=F32) + param(0, g))
        )
        rate = jnp.exp(param(1, g))
        logs = []
        for t in range(props):
            log = -rate * dt[t]
            logs.append(log if t == 0 else logs[-1] + log)
        y = []
        for t in range(props):
            row = jnp.exp(logs[t]) * carried[t] + param(2, g) * x[t]
            for s in range(t + 1):
                score = jnp.sum(c[t] * b[s], axis=-1, keepdims=True)
                weight = dt[s] if s == t else jnp.exp(logs[t] - logs[s]) * dt[s]
                row = row + (score * weight) * x[s]
            y.append(row)
        gated = jnp.concatenate(y, axis=0) * silu(gate)
        mean = jnp.sum(gated * gated, axis=-1, keepdims=True) * (1.0 / gw)
        ys[g][me] = (gated * lax.rsqrt(mean + EPSILON) * param(3, g)).astype(BF16)
        for step in range(1, far):
            z = lax.rem(h + step, far)
            send(ys[g].at[me], ys[g].at[me], y_sem.at[g, me], z * near + l, tp)
        for step in range(1, near):
            k = lax.rem(l + step, near)
            send(ys[g].at[me], ys[g].at[me], y_sem.at[g, me], h * near + k, tp)

    def forward(g):
        for step in range(1, far):
            block = lax.rem(h + far - step, far) * near + l
            arrive(ys[g].at[block], y_sem.at[g, block])
            for side in range(1, near):
                k = lax.rem(l + side, near)
                send(ys[g].at[block], ys[g].at[block], y_sem.at[g, block], h * near + k, tp)

    def output(g):
        for side in range(1, near):
            k = lax.rem(l + near - side, near)
            for step in range(far):
                block = lax.rem(h + far - step, far) * near + k
                arrive(ys[g].at[block], y_sem.at[g, block])
        if g == 0:
            wout_load.wait()
        term = jnp.dot(
            ys[g][...].reshape(n_kv * rows, gw), wout[span(g, gw), :], preferred_element_type=F32
        )
        if g == 0:
            acc[...] = term
        else:
            acc[...] += term

    lag = {"root": -1, "collect": 2, "advance": 3, "forward": 4, "output": 5}
    for i in range(G + max(lag.values())):
        if i < G:
            project(i)
        if 0 < i + 1 < G:
            stores.append(root(i + 1))
        for name, stage_fn in (
            ("collect", collect), ("advance", advance), ("forward", forward), ("output", output),
        ):
            g = i - lag[name]
            if 0 <= g < G:
                stage_fn(g)

    cols = d.out_cols
    mine[...] = acc[...].astype(BF16).reshape(n_kv, rows, cols)
    per = n_kv // n_tp
    side, place = lax.div(me, per), lax.rem(me, per)
    for step in range(n_kv):
        k = lax.rem(me + step, n_kv)
        send(
            mine.at[k], parts.at[tp, place], m_sem.at[tp, place], k, side,
            (side != tp) if step == 0 else None,
        )

    @pl.when(side == tp)
    def _():
        parts[tp, place] = mine[me]

    for t in range(n_tp):
        for k in range(per):
            arrive(
                parts.at[t, k], m_sem.at[t, k], jnp.logical_or(t != tp, tp * per + k != me)
            )
    for k in range(per):
        value = parts[0, k].astype(F32)
        for t in range(1, n_tp):
            value = value + parts[t, k].astype(F32)
        mixed[:, span(k, cols)] = value.astype(BF16)
    for copy, cond in sends:
        if cond is None:
            copy.wait_send()
        else:
            pl.when(cond)(copy.wait_send)
    for copy in stores:
        copy.wait()


def mixer(d, args):
    G, near, far, rows, n_kv = d.groups, d.near, d.far, d.rows, d.n_kv
    dma = pltpu.SemaphoreType.DMA
    vmem, any_ = pl.BlockSpec(memory_space=pltpu.VMEM), pl.BlockSpec(memory_space=pl.ANY)

    def each(shape):
        return [pltpu.VMEM(shape(g), BF16) for g in range(G)]

    scratch = (
        each(lambda g: (near, d.depth, d.cols(g)))
        + each(lambda g: (near, d.depth, d.cols(g)))
        + each(lambda g: (far, near, rows, d.cols(g)))
        + each(lambda g: (far, near, rows, d.cols(g)))
        + each(lambda g: (near, rows, d.cols(g)))
        + each(lambda g: (near, rows, d.cols(g)))
        + each(lambda g: (d.gw, d.seqs * STATE_DIM))
        + each(lambda g: (n_kv, rows, d.gw))
    )
    nb = d.feats // d.block
    hpad = -(-d.heads // LANES) * LANES
    per = n_kv // d.n_tp
    n_send = (
        nb * d.n_tp + d.n_tp - 1 + near - 1
        + G * (2 * (near - 1) + far - 1)
        + G * (far - 1 + (near - 1) * far)
        + n_kv
    )
    n_local = sum(near * (3 if d.thin(g) else 2) for g in range(G)) + 2 * G + 1
    scratch = scratch + [
        pltpu.VMEM((nb, rows, d.block), BF16),
        pltpu.VMEM((near, far, rows, d.block), BF16),
        pltpu.VMEM((d.n_tp, rows, hpad + LANES), F32),
        pltpu.VMEM((d.n_tp, rows, hpad + LANES), F32),
        pltpu.VMEM((d.seqs, G * d.gw, STATE_DIM), F32),
        pltpu.VMEM((G * d.gw, d.out_cols), BF16),
        pltpu.VMEM((n_kv * rows, d.out_cols), F32),
        pltpu.VMEM((n_kv, rows, d.out_cols), BF16),
        pltpu.VMEM((d.n_tp, per, rows, d.out_cols), BF16),
        dma((n_send,)), dma((G, near)), dma((far,)), dma((near,)), dma((d.n_tp,)),
        dma((G, far)), dma((G, near)), dma((G, n_kv)), dma((d.n_tp, per)), dma((n_local,)),
    ]
    specs = [vmem] * len(args)
    for i in (2, 3, 4, 5, 11, 12):
        specs[i] = any_
    past_rows = args[13].shape[0]
    out_shape = [
        jax.ShapeDtypeStruct((rows, d.feats), BF16),
        jax.ShapeDtypeStruct((d.seqs, G * d.gw, STATE_DIM), F32),
        jax.ShapeDtypeStruct((past_rows, d.seqs, G * d.gw), BF16),
        jax.ShapeDtypeStruct((past_rows, d.seqs, G * STATE_DIM), BF16),
        jax.ShapeDtypeStruct((past_rows, d.seqs, G * STATE_DIM), BF16),
        jax.ShapeDtypeStruct((rows, d.heads), BF16),
    ]
    return pl.pallas_call(
        functools.partial(mixer_kernel, d),
        out_shape=out_shape,
        in_specs=specs,
        out_specs=[vmem, any_, vmem, vmem, vmem, vmem],
        scratch_shapes=scratch,
        compiler_params=pltpu.CompilerParams(collective_id=0, has_side_effects=True),
        name="mixer",
    )(*args)


def on_device(
    tokens, input_gain, gate_weight, value_weight, write_weight, read_weight, step_weight,
    conv_value, conv_write, conv_read, step_bias, decay_log, skip_gain, output_gain, out_weight,
    base_state, past_value, past_write, past_read, past_step, accepted,
):
    seqs, props, feats = tokens.shape
    n_kv, n_tp = lax.axis_size("kv"), lax.axis_size("tp")
    depth, inner = gate_weight.shape
    groups = write_weight.shape[1] // STATE_DIM
    heads = step_bias.shape[0]
    gw = inner // groups
    near = near_size(n_kv, gw)
    d = Dims(
        far=n_kv // near, near=near, n_tp=n_tp, seqs=seqs, props=props,
        taps=conv_value.shape[0], width=feats * n_tp, feats=feats, depth=depth, groups=groups,
        gw=gw, heads=heads, out_cols=out_weight.shape[1],
    )

    def major(item):
        return item.transpose(1, 0, 2)

    def per_head(item):
        return jnp.repeat(item, inner // heads)

    head_p = jnp.stack([per_head(step_bias), per_head(decay_log), per_head(skip_gain), output_gain])
    mixed, root, next_v, next_b, next_c, next_s = mixer(
        d,
        (
            major(tokens).reshape(d.rows, feats),
            input_gain.reshape(1, d.width),
            gate_weight, value_weight, write_weight, read_weight,
            step_weight.T,
            conv_value, conv_write, conv_read,
            head_p,
            out_weight,
            base_state.reshape(seqs, inner, STATE_DIM),
            major(past_value), major(past_write), major(past_read),
            major(past_step).reshape(d.rows, heads),
            accepted.reshape(seqs, 1),
        ),
    )
    return (
        major(mixed.reshape(props, seqs, feats)),
        root.reshape(base_state.shape),
        major(next_v), major(next_b), major(next_c),
        major(next_s.reshape(props, seqs, heads)),
    )


def solution(mesh):
    split = P("kv", None, "tp")
    weight = P("kv", "tp")
    state = P("kv", "tp", None, None)
    return jax.shard_map(
        on_device,
        mesh=mesh,
        in_specs=(
            split, P(), weight, weight, weight, weight, P(),
            P(None, "tp"), P(None, "tp"), P(None, "tp"),
            P("tp"), P("tp"), P("tp"), P("tp"),
            P("tp", "kv"),
            state, split, split, split, split, P("kv"),
        ),
        out_specs=(split, state, split, split, split, split),
        check_vma=False,
    )
```

time: 109 us -> 74.3 us (0.68)
  Pallas kernels: 77.7 us -> 56.1 us
  matrix products: 10.1 us -> 0 us
  other arithmetic: 5.76 us -> 1.35 us
  local copies, waits for them, and re-layouts: 11.6 us -> 15.8 us
  blocking collectives: 2.34 us -> 0 us
    pallas_call x2 -> x1, Pallas kernels: 77.7 us -> 56.1 us  [mixer(): pl.pallas_call(functools.partial(mixer_kernel, d), out_shape=out_shape, i...]
    dot_general x4 -> x0, matrix products: 10.1 us -> none  [the longest x1 5.77 us: advance(): jnp.einsum('sh,shp,shn->hpn', weight_now, prev_x, prev_b, precision=highest)]
    all_gather x1 -> x0, blocking collectives: 2.34 us -> none  [on_device(): whole = lax.all_gather(tokens, 'tp', axis=2, tiled=True)]
    gather x6 -> x0, local copies, waits for them, and re-layouts: 2.16 us -> none  [the longest x2 0.86 us: advance(): lax.dynamic_slice_in_dim(past_x, taken, CONV_W - 1, 0)]
    reshape x7 -> x5, local copies, waits for them, and re-layouts: 2.49 us -> 4.63 us  [the longest x2 1.41 us: on_device(): mixed.reshape(props, seqs, feats)]
    broadcast_in_dim x3, local copies, waits for them, and re-layouts: 0.11 us -> 2.18 us  [per_head(): return jnp.repeat(item, inner // heads)]
    transpose x0 -> x2, local copies, waits for them, and re-layouts: none -> 2.06 us  [major(): return item.transpose(1, 0, 2)]
    transpose x2 -> x0, other arithmetic: 1.86 us -> none  [the longest x1 1.12 us: on_device(): wide = jnp.concatenate(cut[:2], axis=2).transpose(1, 0, 2)]
where the time goes in v1:
time: 74.3 us; the launch traced here: 73.9 us
  Pallas kernels  56.1 us (76%)
  local copies, waits for them, and re-layouts  15.8 us (21%)
  other arithmetic  1.35 us (2%)
    pallas_call x1, Pallas kernels, mixer(): pl.pallas_call(functools.partial(mixer_kernel, d), out_shape=out_shape, i...  56.1 us
    unnamed x10, local copies, waits for them, and re-layouts  6.7 us
    broadcast_in_dim x3, local copies, waits for them, and re-layouts, per_head(): return jnp.repeat(item, inner // heads)  2.18 us
    transpose x2, local copies, waits for them, and re-layouts, major(): return item.transpose(1, 0, 2)  2.06 us

profile of v1, /device:TPU:0, one launch (start us, length us, event | category | flops | bytes accessed | tf_op | source)
XLA Modules:
  0.0 73.9 jit_solution(3602945761377936655)
XLA Ops:
  0.6 1.3 %copy.29.refs_17_ = s32[4,1]{1,0:T(4,128)} copy(s32[4,1]{0,1:T(1,128)} %bitcast.39) | data formatting | bytes 32 | tf_op jit(solution)/shard_map/reshape | solution.py:582
  1.9 1.3 %copy.28 = bf16[4,4,32]{2,1,0:T(4,128)(2,1)} copy(bf16[4,4,32]{2,0,1:T(4,128)(2,1)} %bitcast.36) | data formatting | bytes 2048 | tf_op jit(solution)/shard_map/transpose | solution.py:563
  3.2 0.7 broadcast_in_dim.9
  4.0 0.1 stack_reshape.9
  4.0 0.7 broadcast_in_dim.10
  4.8 0.1 stack_reshape.10
  4.8 0.7 broadcast_in_dim.11
  5.6 0.1 stack_reshape.11
  5.7 1.3 %pad_maximum_fusion.refs_10_ = f32[4,2048]{1,0:T(4,128)} fusion(f32[1,2048]{1,0:T(1,128)} %bitcast.35, f32[1,2048]{1,0:T(1,128)S(1)} %stack_reshape.11, f32[1,2048]{1,0:T(1,128)S(1)} %stack_reshape.10, f32[1,2048]{1,0:T(1,128)S(1)} %stack_reshape.9), kind=kLoop, calls=%fused_computation | loop fusion | flops 24576 | bytes 65536 | tf_op jit(solution)/shard_map/stack | solution.py:568
  7.0 0.8 %copy.27 = bf16[4,4,1024]{2,1,0:T(4,128)(2,1)S(1)} copy(bf16[4,4,1024]{2,0,1:T(4,128)(2,1)} %bitcast.27) | data formatting | bytes 65536 | tf_op jit(solution)/shard_map/transpose | solution.py:563
  7.8 0.6 reshape.36.refs_0_
  8.4 56.1 %mixer.1 = (bf16[16,1024]{1,0:T(8,128)(2,1)}, f32[4,2048,128]{2,1,0:T(8,128)}, bf16[7,4,2048]{2,1,0:T(4,128)(2,1)}, bf16[7,4,512]{2,1,0:T(4,128)(2,1)}, bf16[7,4...) custom-call(bf16[16,1024]{1,0:T(8,128)(2,1)} %reshape.36.refs_0_, f32[1,2048]{1,0:T(1,128)} %bitcast.34, ...), custom_call_target="tpu_custom_call" | custom-call | tf_op jit(solution)/shard_map/mixer/pallas_call | solution.py:533
  64.5 0.8 %reshape.41 = bf16[4,4,1024]{2,1,0:T(4,128)(2,1)S(1)} reshape(bf16[16,1024]{1,0:T(8,128)(2,1)} %get-tuple-element.12) | data formatting | bytes 65536 | tf_op jit(solution)/shard_map/reshape | solution.py:586
  65.3 0.6 copy.34
  65.9 1.3 %copy.35 = bf16[4,4,32]{2,0,1:T(4,128)(2,1)} copy(bf16[4,4,32]{2,1,0:T(4,128)(2,1)} %bitcast.38) | data formatting | bytes 2048 | tf_op jit(solution)/shard_map/reshape | solution.py:589
  67.2 0.0 copy-start
  67.2 0.0 copy-start.2
  67.2 0.0 copy-start.1
  67.2 4.8 %copy.40 = f32[4,32,64,128]{3,2,1,0:T(8,128)} copy(f32[4,32,64,128]{3,2,1,0:T(8,128)} %bitcast.23) | data formatting | bytes 8388608
  72.0 0.0 copy-done
  72.0 0.6 copy.41
  72.7 0.0 copy-done.2
  72.7 0.6 copy.42
  73.3 0.0 copy-done.1
  73.3 0.6 copy.43
Async XLA Ops:
  67.2 4.8 %copy-start = (bf16[7,4,2048]{2,1,0:T(4,128)(2,1)S(1)}, bf16[7,4,2048]{2,1,0:T(4,128)(2,1)}, u32[]{:S(2)}) copy-start(bf16[7,4,2048]{2,1,0:T(4,128)(2,1)} %get-tuple-element.14) | copy-start | bytes 344068
  67.2 5.5 %copy-start.2 = (bf16[7,4,512]{2,1,0:T(4,128)(2,1)S(1)}, bf16[7,4,512]{2,1,0:T(4,128)(2,1)}, u32[]{:S(2)}) copy-start(bf16[7,4,512]{2,1,0:T(4,128)(2,1)} %get-tuple-element.15) | copy-start | bytes 86020
  67.2 6.1 %copy-start.1 = (bf16[7,4,512]{2,1,0:T(4,128)(2,1)S(1)}, bf16[7,4,512]{2,1,0:T(4,128)(2,1)}, u32[]{:S(2)}) copy-start(bf16[7,4,512]{2,1,0:T(4,128)(2,1)} %get-tuple-element.16) | copy-start | bytes 86020

commit v2 on v1

--- a/solution.py
+++ b/solution.py
@@ -10,6 +10,7 @@
 
 STATE_DIM = 128
 LANES = 128
+SMALL = 21
 EPSILON = 1e-06
 MESH = pl.DeviceIdType.MESH
 F32 = jnp.float32
@@ -99,39 +100,53 @@
 
 
 def mixer_kernel(d, *refs):
-    (
-        tok, gain, gate_w, value_w, write_w, read_w, step_w, conv_v, conv_b, conv_c, head_p,
-        wout_h, base_h, past_v, past_b, past_c, past_s, taken_ref,
-    ) = refs[:18]
-    mixed, root_h, next_v, next_b, next_c, next_s = refs[18:24]
-    rest = list(refs[24:])
+    gate_w, value_w, write_w, read_w, wout_h, base_h = refs[:6]
+    small = refs[6:SMALL]
+    mixed, base_v, next_v, next_b, next_c, next_s = refs[SMALL : SMALL + 6]
+    rest = list(refs[SMALL + 6 :])
     G = d.groups
     stage, wbuf, zmine, zin, red, back, rootb, ys = (rest[i * G : (i + 1) * G] for i in range(8))
     (
-        xq, xs, pt_mine, pt_in, base_v, wout, acc, mine, parts,
+        xq, xs, pt_mine, pt_in, wout, acc, mine, parts,
         ssem, w_sem, xz_sem, xp_sem, pt_sem, z_sem, b_sem, y_sem, m_sem, l_sem,
-    ) = rest[8 * G :]
+    ) = rest[8 * G : 8 * G + 18]
+    held = rest[8 * G + 18 :]
+    (
+        tok, gain, step_w, conv_v, conv_b, conv_c, bias_r, decay_r, skip_r, gain_out,
+        past_v, past_b, past_c, past_s, taken_ref,
+    ) = held
     far, near, n_tp, rows, S, N = d.far, d.near, d.n_tp, d.rows, d.seqs, STATE_DIM
     n_kv, part, gw, props = d.n_kv, d.part, d.gw, d.props
     me, tp = lax.axis_index("kv"), lax.axis_index("tp")
     h, l = lax.div(me, near), lax.rem(me, near)
 
-    total = n_kv * n_tp
-    flat = me * n_tp + tp
     barrier = pltpu.get_barrier_semaphore()
 
-    def greet(step, carry):
-        other = lax.rem(flat + step, total)
-        pl.semaphore_signal(
-            barrier,
-            inc=1,
-            device_id={"kv": lax.div(other, n_tp), "tp": lax.rem(other, n_tp)},
-            device_id_type=MESH,
-        )
-        return carry
-
-    lax.fori_loop(1, total, greet, 0)
-
+    def greet(kv, t):
+        pl.semaphore_signal(barrier, inc=1, device_id={"kv": kv, "tp": t}, device_id_type=MESH)
+
+    for step in range(1, near):
+        greet(h * near + lax.rem(l + step, near), tp)
+    for t in range(n_tp):
+        for step in range(1, far):
+            greet(lax.rem(h + step, far) * near + l, t)
+    for step in range(1, n_tp):
+        greet(me, lax.rem(tp + step, n_tp))
+    greeted = near - 1 + (far - 1) * n_tp + n_tp - 1
+
+    class Mark:
+        scope = None
+
+        def __call__(self, name):
+            if self.scope is not None:
+                self.scope.__exit__(None, None, None)
+            self.scope = None
+            if name is not None:
+                self.scope = jax.named_scope(name)
+                self.scope.__enter__()
+
+    mark = Mark()
+    mark("prologue")
     used = []
 
     def local(src, dst):
@@ -140,6 +155,7 @@
         used.append(copy)
         return copy
 
+    fetch = [local(src, dst) for src, dst in zip(small, held)]
     units = 2 * G
     staging = []
     for g in range(G):
@@ -183,7 +199,27 @@
 
     nb = d.feats // d.block
     own = pl.multiple_of(tp * d.feats, d.feats)
-    raw = tok[...].astype(F32)
+    for copy in fetch:
+        copy.wait()
+    order = lax.broadcasted_iota(jnp.int32, (rows, rows), 0)
+    other = lax.broadcasted_iota(jnp.int32, (rows, rows), 1)
+
+    def shuffle(major, minor):
+        source = lax.rem(order, minor) * major + lax.div(order, minor)
+        return jnp.where(other == source, 1.0, 0.0).astype(BF16)
+
+    to_time, to_seq = shuffle(props, S), shuffle(S, props)
+
+    def time_major(ref):
+        stacked = jnp.concatenate([ref[s].astype(F32) for s in range(S)], axis=0).astype(BF16)
+        return jnp.dot(to_time, stacked, preferred_element_type=F32)
+
+    def put_seq(ref, cols, value):
+        value = jnp.dot(to_seq, value, preferred_element_type=F32)
+        for s in range(S):
+            ref[s, :, cols] = value[s * props : (s + 1) * props].astype(BF16)
+
+    raw = time_major(tok)
     square = jnp.sum(raw * raw, axis=-1, keepdims=True)
     scaled = (raw * gain[:, pl.ds(own, d.feats)]).astype(BF16)
     for q in range(nb):
@@ -198,8 +234,10 @@
         pt_mine[t, :, hpad : hpad + LANES] = jnp.broadcast_to(square, (rows, LANES))
     pt_in[tp] = pt_mine[tp]
 
-    pl.semaphore_wait(barrier, total - 1)
-
+    mark('barrier')
+    pl.semaphore_wait(barrier, greeted)
+
+    mark('tok_send')
     home = lax.div(h, nb)
     for q in range(nb):
         plane = tp * nb + q
@@ -224,7 +262,17 @@
 
     send_weights(0)
 
-    taken = taken_ref[...]
+    diagonal = lax.broadcasted_iota(jnp.int32, (S, S), 0) == lax.broadcasted_iota(
+        jnp.int32, (S, S), 1
+    )
+    taken = jnp.sum(
+        jnp.where(diagonal, taken_ref[...].astype(F32), 0.0), axis=-1, keepdims=True
+    ).astype(jnp.int32)
+    steps_old = time_major(past_s).astype(BF16)
+    head_rows = jnp.concatenate(
+        [bias_r[...], decay_r[...], skip_r[...]] + [jnp.zeros_like(bias_r[...])] * 5, axis=0
+    )
+    params = []
     row_seq = lax.rem(lax.broadcasted_iota(jnp.int32, (rows, N), 0), S)
 
     def spread(g):
@@ -241,7 +289,14 @@
         return [ref[k : k + 1, cols] for k in range(d.taps)]
 
     def param(k, g):
-        return head_p[k : k + 1, span(g, gw)]
+        if g == len(params):
+            params.append(
+                jnp.dot(
+                    head_rows, spread(g).astype(F32), preferred_element_type=F32,
+                    precision=lax.Precision.HIGHEST,
+                )
+            )
+        return params[g][k : k + 1]
 
     def pieces(v):
         return [v[t * S : (t + 1) * S] for t in range(props)]
@@ -250,12 +305,13 @@
         return [ref[i, :, cols].astype(F32) for i in range(ref.shape[0])]
 
     def root(g):
+        mark(f'root{g}')
         loading[g].wait()
         cv, cn = span(g, gw), span(g, N)
         px = [silu(v) for v in conv(old(past_v, cv), taps(conv_v, cv), props)]
         pb = [silu(v) for v in conv(old(past_b, cn), taps(conv_b, cn), props)]
         pd = softplus(
-            jnp.dot(past_s[...], spread(g), preferred_element_type=F32) + param(0, g)
+            jnp.dot(steps_old, spread(g), preferred_element_type=F32) + param(0, g)
         )
         rate = jnp.exp(param(1, g))
         pd = pieces(pd)
@@ -279,10 +335,10 @@
             new = decay[:, s : s + 1] * base_v[s, cv, :] + outer
             base_v[s, cv, :] = new
             rootb[g][:, span(s, N)] = new.astype(BF16)
-        return local(base_v.at[:, cv], root_h.at[:, cv])
-
-    stores = [root(0)]
-
+
+    root(0)
+
+    mark('tokz_wait')
     for k in range(far):
         arrive(
             xs.at[l, k], xz_sem.at[k], jnp.logical_or(h != k, home != tp)
@@ -292,6 +348,7 @@
     for g in range(1, G):
         send_weights(g)
 
+    mark('scale')
     for step in range(1, n_tp):
         t = lax.rem(tp + n_tp - step, n_tp)
         arrive(pt_in.at[t], pt_sem.at[t])
@@ -300,17 +357,20 @@
         joined = joined + pt_in[t]
     scale = lax.rsqrt(joined[:, hpad : hpad + LANES] * (1.0 / d.width) + EPSILON)
     step_now = (joined[:, 0 : d.heads] * scale[:, 0 : d.heads]).astype(BF16)
-    next_s[...] = step_now
-
+    put_seq(next_s, slice(None), step_now)
+
+    mark('tokp_wait')
     for step in range(1, near):
         k = lax.rem(l + near - step, near)
         arrive(xs.at[k], xp_sem.at[k])
 
     def project(g):
+        mark(f'w_wait{g}')
         wbuf[g][l] = stage[g][l]
         for step in range(1, near):
             k = lax.rem(l + near - step, near)
             arrive(wbuf[g].at[k], w_sem.at[g, k])
+        mark(f'matmul{g}')
         cols = d.cols(g)
         product = jnp.dot(
             xs[...].reshape(n_kv * rows, d.block),
@@ -326,6 +386,7 @@
             send(zmine[g].at[z], zin[g].at[h], z_sem.at[g, h], z * near + l, tp)
 
     def collect(g):
+        mark(f'z_wait{g}')
         value = zmine[g][h].astype(F32)
         for step in range(1, far):
             z = lax.rem(h + far - step, far)
@@ -341,10 +402,12 @@
         return (piece.astype(F32) * scale).astype(BF16).astype(F32)
 
     def advance(g):
+        mark(f'b_wait{g}')
         for step in range(1, near):
             k = lax.rem(l + near - step, near)
             arrive(back[g].at[k], b_sem.at[g, k])
         cv, cn = span(g, gw), span(g, N)
+        mark(f'advance{g}')
         gate = jnp.concatenate([rounded(back[g][k, :, 0:part]) for k in range(near)], axis=1)
         value = jnp.concatenate(
             [rounded(back[g][k, :, part : 2 * part]) for k in range(near)], axis=1
@@ -398,7 +461,7 @@
             y.append(row)
         gated = jnp.concatenate(y, axis=0) * silu(gate)
         mean = jnp.sum(gated * gated, axis=-1, keepdims=True) * (1.0 / gw)
-        ys[g][me] = (gated * lax.rsqrt(mean + EPSILON) * param(3, g)).astype(BF16)
+        ys[g][me] = (gated * lax.rsqrt(mean + EPSILON) * gain_out[:, cv]).astype(BF16)
         for step in range(1, far):
             z = lax.rem(h + step, far)
             send(ys[g].at[me], ys[g].at[me], y_sem.at[g, me], z * near + l, tp)
@@ -407,6 +470,7 @@
             send(ys[g].at[me], ys[g].at[me], y_sem.at[g, me], h * near + k, tp)
 
     def forward(g):
+        mark(f'yz_wait{g}')
         for step in range(1, far):
             block = lax.rem(h + far - step, far) * near + l
             arrive(ys[g].at[block], y_sem.at[g, block])
@@ -415,6 +479,7 @@
                 send(ys[g].at[block], ys[g].at[block], y_sem.at[g, block], h * near + k, tp)
 
     def output(g):
+        mark(f'y_wait{g}')
         for side in range(1, near):
             k = lax.rem(l + near - side, near)
             for step in range(far):
@@ -422,6 +487,7 @@
                 arrive(ys[g].at[block], y_sem.at[g, block])
         if g == 0:
             wout_load.wait()
+        mark(f'out{g}')
         term = jnp.dot(
             ys[g][...].reshape(n_kv * rows, gw), wout[span(g, gw), :], preferred_element_type=F32
         )
@@ -430,19 +496,18 @@
         else:
             acc[...] += term
 
-    lag = {"root": -1, "collect": 2, "advance": 3, "forward": 4, "output": 5}
-    for i in range(G + max(lag.values())):
-        if i < G:
-            project(i)
-        if 0 < i + 1 < G:
-            stores.append(root(i + 1))
-        for name, stage_fn in (
-            ("collect", collect), ("advance", advance), ("forward", forward), ("output", output),
-        ):
-            g = i - lag[name]
-            if 0 <= g < G:
-                stage_fn(g)
-
+    stages = (
+        (project, 0.0), (collect, 5.0), (advance, 9.0), (forward, 13.0), (output, 25.0),
+    )
+    order_of = sorted(
+        (start + 3.3 * g, i, g) for i, (_, start) in enumerate(stages) for g in range(G)
+    )
+    for _, i, g in order_of:
+        stages[i][0](g)
+        if i == 0 and g + 1 < G:
+            root(g + 1)
+
+    mark('final_send')
     cols = d.out_cols
     mine[...] = acc[...].astype(BF16).reshape(n_kv, rows, cols)
     per = n_kv // n_tp
@@ -458,6 +523,7 @@
     def _():
         parts[tp, place] = mine[me]
 
+    mark('final_wait')
     for t in range(n_tp):
         for k in range(per):
             arrive(
@@ -467,20 +533,20 @@
         value = parts[0, k].astype(F32)
         for t in range(1, n_tp):
             value = value + parts[t, k].astype(F32)
-        mixed[:, span(k, cols)] = value.astype(BF16)
+        put_seq(mixed, span(k, cols), value.astype(BF16))
+    mark('drain')
     for copy, cond in sends:
         if cond is None:
             copy.wait_send()
         else:
             pl.when(cond)(copy.wait_send)
-    for copy in stores:
-        copy.wait()
+    mark(None)
 
 
 def mixer(d, args):
     G, near, far, rows, n_kv = d.groups, d.near, d.far, d.rows, d.n_kv
     dma = pltpu.SemaphoreType.DMA
-    vmem, any_ = pl.BlockSpec(memory_space=pltpu.VMEM), pl.BlockSpec(memory_space=pl.ANY)
+    vmem, hbm = pl.BlockSpec(memory_space=pltpu.VMEM), pl.BlockSpec(memory_space=pltpu.HBM)
 
     def each(shape):
         return [pltpu.VMEM(shape(g), BF16) for g in range(G)]
@@ -504,13 +570,12 @@
         + G * (far - 1 + (near - 1) * far)
         + n_kv
     )
-    n_local = sum(near * (3 if d.thin(g) else 2) for g in range(G)) + 2 * G + 1
+    n_local = sum(near * (3 if d.thin(g) else 2) for g in range(G)) + G + 1 + len(args) - 6
     scratch = scratch + [
         pltpu.VMEM((nb, rows, d.block), BF16),
         pltpu.VMEM((near, far, rows, d.block), BF16),
         pltpu.VMEM((d.n_tp, rows, hpad + LANES), F32),
         pltpu.VMEM((d.n_tp, rows, hpad + LANES), F32),
-        pltpu.VMEM((d.seqs, G * d.gw, STATE_DIM), F32),
         pltpu.VMEM((G * d.gw, d.out_cols), BF16),
         pltpu.VMEM((n_kv * rows, d.out_cols), F32),
         pltpu.VMEM((n_kv, rows, d.out_cols), BF16),
@@ -518,27 +583,50 @@
         dma((n_send,)), dma((G, near)), dma((far,)), dma((near,)), dma((d.n_tp,)),
         dma((G, far)), dma((G, near)), dma((G, n_kv)), dma((d.n_tp, per)), dma((n_local,)),
     ]
-    specs = [vmem] * len(args)
-    for i in (2, 3, 4, 5, 11, 12):
-        specs[i] = any_
-    past_rows = args[13].shape[0]
-    out_shape = [
-        jax.ShapeDtypeStruct((rows, d.feats), BF16),
-        jax.ShapeDtypeStruct((d.seqs, G * d.gw, STATE_DIM), F32),
-        jax.ShapeDtypeStruct((past_rows, d.seqs, G * d.gw), BF16),
-        jax.ShapeDtypeStruct((past_rows, d.seqs, G * STATE_DIM), BF16),
-        jax.ShapeDtypeStruct((past_rows, d.seqs, G * STATE_DIM), BF16),
-        jax.ShapeDtypeStruct((rows, d.heads), BF16),
-    ]
+    scratch = scratch + [pltpu.VMEM(item.shape, item.dtype) for item in args[6:]]
+    past_v, past_b, past_c = (item.shape for item in args[-5:-2])
     return pl.pallas_call(
         functools.partial(mixer_kernel, d),
-        out_shape=out_shape,
-        in_specs=specs,
-        out_specs=[vmem, any_, vmem, vmem, vmem, vmem],
+        out_shape=[
+            pltpu.VMEM((d.seqs, d.props, d.feats), BF16),
+            pltpu.VMEM((d.seqs, G * d.gw, STATE_DIM), F32),
+            pltpu.VMEM(past_v, BF16),
+            pltpu.VMEM(past_b, BF16),
+            pltpu.VMEM(past_c, BF16),
+            pltpu.VMEM((d.seqs, d.props, d.heads), BF16),
+        ],
+        in_specs=[hbm] * len(args),
+        out_specs=[vmem] * 6,
         scratch_shapes=scratch,
-        compiler_params=pltpu.CompilerParams(collective_id=0, has_side_effects=True),
+        compiler_params=pltpu.CompilerParams(
+            collective_id=0, has_side_effects=True, vmem_limit_bytes=24 * 2**20
+        ),
         name="mixer",
-    )(*args)
+    )(*(pltpu.with_memory_space_constraint(item, pltpu.HBM) for item in args))
+
+
+def store_kernel(count, *refs):
+    sem = refs[-1]
+    copies = [
+        pltpu.make_async_copy(refs[i], refs[count + i], sem.at[i]) for i in range(count)
+    ]
+    for copy in copies:
+        copy.start()
+    for copy in copies:
+        copy.wait()
+
+
+def store(items):
+    count = len(items)
+    return pl.pallas_call(
+        functools.partial(store_kernel, count),
+        out_shape=[jax.ShapeDtypeStruct(item.shape, item.dtype) for item in items],
+        in_specs=[pl.BlockSpec(memory_space=pltpu.VMEM)] * count,
+        out_specs=[pl.BlockSpec(memory_space=pltpu.HBM)] * count,
+        scratch_shapes=[pltpu.SemaphoreType.DMA((count,))],
+        compiler_params=pltpu.CompilerParams(vmem_limit_bytes=2**20),
+        name="store",
+    )(*items)
 
 
 def on_device(
@@ -562,31 +650,22 @@
     def major(item):
         return item.transpose(1, 0, 2)
 
-    def per_head(item):
-        return jnp.repeat(item, inner // heads)
-
-    head_p = jnp.stack([per_head(step_bias), per_head(decay_log), per_head(skip_gain), output_gain])
-    mixed, root, next_v, next_b, next_c, next_s = mixer(
+    def line(item):
+        return item.reshape(1, item.shape[0])
+
+    outs = mixer(
         d,
         (
-            major(tokens).reshape(d.rows, feats),
-            input_gain.reshape(1, d.width),
-            gate_weight, value_weight, write_weight, read_weight,
-            step_weight.T,
-            conv_value, conv_write, conv_read,
-            head_p,
-            out_weight,
+            gate_weight, value_weight, write_weight, read_weight, out_weight,
             base_state.reshape(seqs, inner, STATE_DIM),
-            major(past_value), major(past_write), major(past_read),
-            major(past_step).reshape(d.rows, heads),
-            accepted.reshape(seqs, 1),
+            tokens, line(input_gain), step_weight.T, conv_value, conv_write, conv_read,
+            line(step_bias), line(decay_log), line(skip_gain), line(output_gain),
+            major(past_value), major(past_write), major(past_read), past_step, line(accepted),
         ),
     )
+    mixed, root, next_v, next_b, next_c, next_s = store(outs)
     return (
-        major(mixed.reshape(props, seqs, feats)),
-        root.reshape(base_state.shape),
-        major(next_v), major(next_b), major(next_c),
-        major(next_s.reshape(props, seqs, heads)),
+        mixed, root.reshape(base_state.shape), major(next_v), major(next_b), major(next_c), next_s,
     )
 
 

time: 74.3 us -> 54.8 us (0.74)
  local copies, waits for them, and re-layouts: 15.8 us -> 0 us
  Pallas kernels: 56.1 us -> 54 us
  other arithmetic: 1.35 us -> 0 us
    unnamed x10 -> x0, local copies, waits for them, and re-layouts: 6.7 us -> none
    reshape x5 -> x0, local copies, waits for them, and re-layouts: 4.63 us -> none  [the longest x2 1.41 us: on_device(): mixed.reshape(props, seqs, feats)]
    broadcast_in_dim x3 -> x0, local copies, waits for them, and re-layouts: 2.18 us -> none  [per_head(): return jnp.repeat(item, inner // heads)]
    pallas_call x1 -> x2, Pallas kernels: 56.1 us -> 54 us  [the longest x1 51.9 us: mixer(): pl.pallas_call(functools.partial(mixer_kernel, d), out_shape=[pltpu.VMEM(...]
    transpose x2 -> x0, local copies, waits for them, and re-layouts: 2.06 us -> none  [major(): return item.transpose(1, 0, 2)]
    another operation x1 -> x0, other arithmetic: 1.35 us -> none  [on_device(): jnp.stack([per_head(step_bias), per_head(decay_log), per_head(skip_gain),...]
where the time goes in v2:
time: 54.8 us; the launch traced here: 54.6 us
  Pallas kernels  54 us (99%)
  between operations  0.65 us (1%)
    pallas_call x1, Pallas kernels, mixer(): pl.pallas_call(functools.partial(mixer_kernel, d), out_shape=[pltpu.VMEM(...  51.9 us
    pallas_call x1, Pallas kernels, store(): pl.pallas_call(functools.partial(store_kernel, count), out_shape=[jax.Sha...  2.1 us

profile of v2, /device:TPU:0, one launch (start us, length us, event | category | flops | bytes accessed | tf_op | source)
XLA Modules:
  0.0 54.6 jit_solution(9848797491068051499)
XLA Ops:
  0.6 51.9 %mixer.1 = (bf16[4,4,1024]{2,1,0:T(4,128)(2,1)S(1)}, f32[4,2048,128]{2,1,0:T(8,128)S(1)}, bf16[7,4,2048]{2,1,0:T(4,128)(2,1)S(1)}, bf16[7,4,512]{2,1,0:T(4,128)(...) custom-call(bf16[128,2048]{1,0:T(8,128)(2,1)} %refs_0_.1, bf16[128,2048]{1,0:T(8,128)(2,1)} %refs_1_.1, ...), custom_call_target="tpu_custom_call" | custom-call | tf_op jit(solution)/shard_map/mixer/pallas_call | solution.py:588
  52.5 2.1 %store.1 = (bf16[4,4,1024]{2,1,0:T(4,128)(2,1)}, f32[4,2048,128]{2,1,0:T(8,128)}, bf16[7,4,2048]{2,1,0:T(4,128)(2,1)}, bf16[7,4,512]{2,1,0:T(4,128)(2,1)}, bf16[...) custom-call(bf16[4,4,1024]{2,1,0:T(4,128)(2,1)S(1)} %get-tuple-element.18.refs_0_, ...), custom_call_target="tpu_custom_call" | custom-call | tf_op jit(solution)/shard_map/store/pallas_call | solution.py:621

commit v3 on v2

--- a/solution.py
+++ b/solution.py
@@ -48,12 +48,8 @@
     def part(self):
         return self.gw // self.near
 
-    @property
-    def every(self):
-        return self.near // 2
-
     def thin(self, g):
-        return g % self.every == 0
+        return g * self.near < 2 * self.groups
 
     def cols(self, g):
         return 2 * self.part + (STATE_DIM if self.thin(g) else 0)
@@ -105,12 +101,15 @@
     mixed, base_v, next_v, next_b, next_c, next_s = refs[SMALL : SMALL + 6]
     rest = list(refs[SMALL + 6 :])
     G = d.groups
-    stage, wbuf, zmine, zin, red, back, rootb, ys = (rest[i * G : (i + 1) * G] for i in range(8))
+    stage, wbuf, zmine, zin, red, back, rootb = (rest[i * G : (i + 1) * G] for i in range(7))
+    ys, rest = rest[7 * G : 8 * G - 1], rest[8 * G - 1 :]
+    last = G - 1
     (
-        xq, xs, pt_mine, pt_in, wout, acc, mine, parts,
-        ssem, w_sem, xz_sem, xp_sem, pt_sem, z_sem, b_sem, y_sem, m_sem, l_sem,
-    ) = rest[8 * G : 8 * G + 18]
-    held = rest[8 * G + 18 :]
+        xq, xs, pt_mine, pt_in, wout, acc, mine, parts, wlast, ylast, mine_l, parts_l,
+        ssem, w_sem, xz_sem, xp_sem, pt_sem, z_sem, b_sem, yz_sem, yp_sem, m_sem,
+        wl_sem, yl_sem, ml_sem, l_sem, g_sem,
+    ) = rest[:27]
+    held = rest[27:]
     (
         tok, gain, step_w, conv_v, conv_b, conv_c, bias_r, decay_r, skip_r, gain_out,
         past_v, past_b, past_c, past_s, taken_ref,
@@ -157,34 +156,43 @@
 
     fetch = [local(src, dst) for src, dst in zip(small, held)]
     units = 2 * G
-    staging = []
     for g in range(G):
-        copies = []
+        def stage_in(src, dst):
+            pltpu.make_async_copy(src, dst, g_sem.at[g]).start()
+
         for k in range(near):
             lo = g * gw + k * part
-            copies.append(local(gate_w.at[:, lo : lo + part], stage[g].at[k, :, 0:part]))
-            copies.append(local(value_w.at[:, lo : lo + part], stage[g].at[k, :, part : 2 * part]))
+            stage_in(gate_w.at[:, lo : lo + part], stage[g].at[k, :, 0:part])
+            stage_in(value_w.at[:, lo : lo + part], stage[g].at[k, :, part : 2 * part])
             if d.thin(g):
-                u = (g // d.every * near + k) % units
+                u = (g * near + k) % units
                 source = (write_w, read_w)[u % 2]
-                copies.append(
-                    local(
-                        source.at[:, u // 2 * N : (u // 2 + 1) * N],
-                        stage[g].at[k, :, 2 * part : 2 * part + N],
-                    )
+                stage_in(
+                    source.at[:, u // 2 * N : (u // 2 + 1) * N],
+                    stage[g].at[k, :, 2 * part : 2 * part + N],
                 )
-        staging.append(copies)
     loading = [
         local(base_h.at[:, g * gw : (g + 1) * gw], base_v.at[:, g * gw : (g + 1) * gw])
         for g in range(G)
     ]
+    wlast_load = local(wout_h.at[last * gw : G * gw], wlast.at[h])
     wout_load = local(wout_h, wout)
 
-    sends = []
-
-    def send(src, dst, recv, kv, t, cond=None):
-        copy = remote(src, dst, ssem.at[len(sends)], recv, kv, t)
-        sends.append((copy, cond))
+    drains = []
+
+    def meter(ref, count):
+        at = len(drains)
+        size = ref if count is None else ref.at[pl.ds(0, count)]
+        drains.append((size, at, None))
+        return at
+
+    def alone(src, cond=None):
+        drains.append((src, len(drains), cond))
+        return len(drains) - 1
+
+    def send(src, dst, recv, kv, t, cond=None, via=None):
+        at = alone(src, cond) if via is None else via
+        copy = remote(src, dst, ssem.at[at], recv, kv, t)
         if cond is None:
             copy.start()
         else:
@@ -196,6 +204,9 @@
             copy.wait_recv()
         else:
             pl.when(cond)(copy.wait_recv)
+
+    def first(ref, count):
+        return ref.at[pl.ds(0, count)]
 
     nb = d.feats // d.block
     own = pl.multiple_of(tp * d.feats, d.feats)
@@ -254,13 +265,28 @@
         send(pt_mine.at[t], pt_in.at[tp], pt_sem.at[tp], me, t)
 
     def send_weights(g):
-        for copy in staging[g]:
-            copy.wait()
+        arrive(stage[g], g_sem.at[g])
+        via = meter(stage[g], near - 1)
         for step in range(1, near):
             k = lax.rem(l + step, near)
-            send(stage[g].at[k], wbuf[g].at[l], w_sem.at[g, l], h * near + k, tp)
+            send(stage[g].at[k], wbuf[g].at[l], w_sem.at[g], h * near + k, tp, via=via)
 
     send_weights(0)
+    wlast_load.wait()
+
+    def inside(z):
+        return jnp.logical_and(z >= 0, z < far)
+
+    def relay(level):
+        for way in (1, -1):
+            z = h - way * level
+            block = lax.rem(z + far, far)
+            if level:
+                arrive(wlast.at[block], wl_sem.at[block], inside(z))
+            if level < far - 1:
+                peer = lax.rem(h + way + far, far) * near + l
+                go = jnp.logical_and(inside(z), inside(h + way))
+                send(wlast.at[block], wlast.at[block], wl_sem.at[block], peer, tp, go)
 
     diagonal = lax.broadcasted_iota(jnp.int32, (S, S), 0) == lax.broadcasted_iota(
         jnp.int32, (S, S), 1
@@ -336,17 +362,28 @@
             base_v[s, cv, :] = new
             rootb[g][:, span(s, N)] = new.astype(BF16)
 
-    root(0)
+    for g in range(max(1, G - 1)):
+        root(g)
 
     mark('tokz_wait')
     for k in range(far):
         arrive(
             xs.at[l, k], xz_sem.at[k], jnp.logical_or(h != k, home != tp)
         )
+    fq = far // n_tp
+
+    def piece(k, t):
+        return xs.at[k, pl.ds(t * fq, fq)]
+
+    via_x = meter(xs, near - 1)
     for step in range(1, near):
-        send(xs.at[l], xs.at[l], xp_sem.at[l], h * near + lax.rem(l + step, near), tp)
+        k = h * near + lax.rem(l + step, near)
+        send(piece(l, tp), piece(l, tp), xp_sem.at[l, tp], k, tp, via=via_x)
     for g in range(1, G):
         send_weights(g)
+    relay(0)
+    if G > 1:
+        root(G - 1)
 
     mark('scale')
     for step in range(1, n_tp):
@@ -362,14 +399,20 @@
     mark('tokp_wait')
     for step in range(1, near):
         k = lax.rem(l + near - step, near)
-        arrive(xs.at[k], xp_sem.at[k])
+        arrive(piece(k, tp), xp_sem.at[k, tp])
+        for side in range(1, n_tp):
+            t = lax.rem(tp + side, n_tp)
+            send(piece(k, tp), piece(k, tp), xp_sem.at[k, tp], me, t, via=via_x)
+    for step in range(1, near):
+        k = lax.rem(l + near - step, near)
+        for side in range(1, n_tp):
+            t = lax.rem(tp + n_tp - side, n_tp)
+            arrive(piece(k, t), xp_sem.at[k, t])
 
     def project(g):
         mark(f'w_wait{g}')
         wbuf[g][l] = stage[g][l]
-        for step in range(1, near):
-            k = lax.rem(l + near - step, near)
-            arrive(wbuf[g].at[k], w_sem.at[g, k])
+        arrive(first(wbuf[g], near - 1), w_sem.at[g])
         mark(f'matmul{g}')
         cols = d.cols(g)
         product = jnp.dot(
@@ -381,31 +424,33 @@
             for z in range(far):
                 at = (k * far + z) * rows
                 zmine[g][z, k] = product[at : at + rows]
-        for step in range(1, far):
+        via = meter(zmine[g], far - 1)
+        for step in reversed(range(1, far)):
             z = lax.rem(h + step, far)
-            send(zmine[g].at[z], zin[g].at[h], z_sem.at[g, h], z * near + l, tp)
+            send(zmine[g].at[z], zin[g].at[h], z_sem.at[g], z * near + l, tp, via=via)
 
     def collect(g):
         mark(f'z_wait{g}')
+        arrive(first(zin[g], far - 1), z_sem.at[g])
         value = zmine[g][h].astype(F32)
         for step in range(1, far):
             z = lax.rem(h + far - step, far)
-            arrive(zin[g].at[z], z_sem.at[g, z])
             value = value + zin[g][z].astype(F32)
         red[g][...] = value.astype(BF16)
         back[g][l] = red[g][l]
+        via = meter(red[g], near - 1)
         for step in range(1, near):
             k = lax.rem(l + step, near)
-            send(red[g].at[k], back[g].at[l], b_sem.at[g, l], h * near + k, tp)
+            send(red[g].at[k], back[g].at[l], b_sem.at[g], h * near + k, tp, via=via)
 
     def rounded(piece):
         return (piece.astype(F32) * scale).astype(BF16).astype(F32)
 
+    via_y = {}
+
     def advance(g):
         mark(f'b_wait{g}')
-        for step in range(1, near):
-            k = lax.rem(l + near - step, near)
-            arrive(back[g].at[k], b_sem.at[g, k])
+        arrive(first(back[g], near - 1), b_sem.at[g])
         cv, cn = span(g, gw), span(g, N)
         mark(f'advance{g}')
         gate = jnp.concatenate([rounded(back[g][k, :, 0:part]) for k in range(near)], axis=1)
@@ -415,7 +460,7 @@
 
         def unit(u):
             j, k = u // near, u % near
-            return rounded(back[j * d.every][k, :, 2 * part : 2 * part + N])
+            return rounded(back[j][k, :, 2 * part : 2 * part + N])
 
         def window(past, now, out, cols):
             before = old(past, cols)
@@ -461,30 +506,36 @@
             y.append(row)
         gated = jnp.concatenate(y, axis=0) * silu(gate)
         mean = jnp.sum(gated * gated, axis=-1, keepdims=True) * (1.0 / gw)
-        ys[g][me] = (gated * lax.rsqrt(mean + EPSILON) * gain_out[:, cv]).astype(BF16)
-        for step in range(1, far):
+        normal = (gated * lax.rsqrt(mean + EPSILON) * gain_out[:, cv]).astype(BF16)
+        if g == last:
+            ylast[l] = normal
+            via = meter(ylast, near - 1)
+            for step in range(1, near):
+                k = lax.rem(l + step, near)
+                send(ylast.at[l], ylast.at[l], yl_sem.at[0], h * near + k, tp, via=via)
+            return
+        ys[g][me] = normal
+        via_y[g] = meter(ys[g], n_kv - 1)
+        for step in reversed(range(1, far)):
             z = lax.rem(h + step, far)
-            send(ys[g].at[me], ys[g].at[me], y_sem.at[g, me], z * near + l, tp)
+            spot = ys[g].at[me]
+            send(spot, spot, yz_sem.at[g], z * near + l, tp, via=via_y[g])
         for step in range(1, near):
             k = lax.rem(l + step, near)
-            send(ys[g].at[me], ys[g].at[me], y_sem.at[g, me], h * near + k, tp)
+            send(spot, spot, yp_sem.at[g], h * near + k, tp, via=via_y[g])
 
     def forward(g):
         mark(f'yz_wait{g}')
+        arrive(first(ys[g], far - 1), yz_sem.at[g])
         for step in range(1, far):
-            block = lax.rem(h + far - step, far) * near + l
-            arrive(ys[g].at[block], y_sem.at[g, block])
+            spot = ys[g].at[lax.rem(h + far - step, far) * near + l]
             for side in range(1, near):
                 k = lax.rem(l + side, near)
-                send(ys[g].at[block], ys[g].at[block], y_sem.at[g, block], h * near + k, tp)
+                send(spot, spot, yp_sem.at[g], h * near + k, tp, via=via_y[g])
 
     def output(g):
         mark(f'y_wait{g}')
-        for side in range(1, near):
-            k = lax.rem(l + near - side, near)
-            for step in range(far):
-                block = lax.rem(h + far - step, far) * near + k
-                arrive(ys[g].at[block], y_sem.at[g, block])
+        arrive(first(ys[g], (near - 1) * far), yp_sem.at[g])
         if g == 0:
             wout_load.wait()
         mark(f'out{g}')
@@ -496,46 +547,90 @@
         else:
             acc[...] += term
 
-    stages = (
-        (project, 0.0), (collect, 5.0), (advance, 9.0), (forward, 13.0), (output, 25.0),
-    )
-    order_of = sorted(
-        (start + 3.3 * g, i, g) for i, (_, start) in enumerate(stages) for g in range(G)
-    )
-    for _, i, g in order_of:
-        stages[i][0](g)
-        if i == 0 and g + 1 < G:
-            root(g + 1)
-
-    mark('final_send')
     cols = d.out_cols
-    mine[...] = acc[...].astype(BF16).reshape(n_kv, rows, cols)
     per = n_kv // n_tp
     side, place = lax.div(me, per), lax.rem(me, per)
-    for step in range(n_kv):
-        k = lax.rem(me + step, n_kv)
-        send(
-            mine.at[k], parts.at[tp, place], m_sem.at[tp, place], k, side,
-            (side != tp) if step == 0 else None,
-        )
-
-    @pl.when(side == tp)
-    def _():
-        parts[tp, place] = mine[me]
+    deep = per // near
+
+    def share():
+        mark('share')
+        mine[...] = acc[...].astype(BF16).reshape(n_kv, rows, cols)
+        via = meter(mine, n_kv - 1)
+        slot = parts.at[tp * per + place]
+        for step in range(1, n_kv):
+            k = lax.rem(me + step, n_kv)
+            send(mine.at[k], slot, m_sem.at[0], k, side, via=via)
+        send(mine.at[me], slot, m_sem.at[0], me, side, side != tp)
+
+        @pl.when(side == tp)
+        def _():
+            parts[tp * per + place] = mine[me]
+
+    def output_last():
+        mark('wl_wait')
+        for level in levels:
+            relay(level)
+        if not last:
+            wout_load.wait()
+        mark('yl_wait')
+        arrive(first(ylast, near - 1), yl_sem.at[0])
+        mark('outl')
+        every = ylast[...].reshape(near * rows, gw)
+        for z in range(far):
+            term = jnp.dot(every, wlast[z], preferred_element_type=F32).astype(BF16)
+            for k in range(near):
+                mine_l[z // deep * near + k, z % deep] = term[k * rows : (k + 1) * rows]
+        via = meter(mine_l, near * n_tp - 1)
+        spot = tp * near + l
+        for step in range(1, near * n_tp):
+            to = lax.rem(spot + step, near * n_tp)
+            send(
+                mine_l.at[to], parts_l.at[spot], ml_sem.at[0],
+                h * near + lax.rem(to, near), lax.div(to, near), via=via,
+            )
+        parts_l[spot] = mine_l[spot]
+
+    plan = (
+        (project, lambda g: 2.75 * g),
+        (collect, lambda g: 8.0 + 3.0 * g if g else 5.6),
+        (advance, lambda g: 12.0 + 2.7 * g if g else 9.0),
+        (forward, lambda g: 17.6 + 1.9 * g),
+    )
+    order_of = sorted(
+        (when(g), i, g)
+        for i, (_, when) in enumerate(plan)
+        for g in range(G if i < 3 else last)
+    )
+    levels = iter(range(1, far))
+    for _, i, g in order_of:
+        plan[i][0](g)
+        if far > 3 and g == last - 1 and i > 1:
+            relay(next(levels))
+
+    for g in range(last):
+        output(g)
+    if last:
+        share()
+    output_last()
 
     mark('final_wait')
-    for t in range(n_tp):
-        for k in range(per):
-            arrive(
-                parts.at[t, k], m_sem.at[t, k], jnp.logical_or(t != tp, tp * per + k != me)
-            )
+    if last:
+        arrive(first(parts, n_kv - 1), m_sem.at[0], side == tp)
+        arrive(parts, m_sem.at[0], side != tp)
+    mark('final_last')
+    arrive(first(parts_l, near * n_tp - 1), ml_sem.at[0])
     for k in range(per):
-        value = parts[0, k].astype(F32)
-        for t in range(1, n_tp):
-            value = value + parts[t, k].astype(F32)
+        value = None
+        for t in range(n_tp):
+            terms = [parts_l[t * near + k % near, k // near]]
+            terms = terms + ([parts[t * per + k]] if last else [])
+            for term in terms:
+                term = term.astype(F32)
+                value = term if value is None else value + term
         put_seq(mixed, span(k, cols), value.astype(BF16))
     mark('drain')
-    for copy, cond in sends:
+    for size, at, cond in drains:
+        copy = remote(size, size, ssem.at[at], l_sem.at[0], me, tp)
         if cond is None:
             copy.wait_send()
         else:
@@ -559,18 +654,13 @@
         + each(lambda g: (near, rows, d.cols(g)))
         + each(lambda g: (near, rows, d.cols(g)))
         + each(lambda g: (d.gw, d.seqs * STATE_DIM))
-        + each(lambda g: (n_kv, rows, d.gw))
+        + each(lambda g: (n_kv, rows, d.gw))[: G - 1]
     )
     nb = d.feats // d.block
     hpad = -(-d.heads // LANES) * LANES
     per = n_kv // d.n_tp
-    n_send = (
-        nb * d.n_tp + d.n_tp - 1 + near - 1
-        + G * (2 * (near - 1) + far - 1)
-        + G * (far - 1 + (near - 1) * far)
-        + n_kv
-    )
-    n_local = sum(near * (3 if d.thin(g) else 2) for g in range(G)) + G + 1 + len(args) - 6
+    n_send = nb * d.n_tp + d.n_tp - 1 + 1 + 3 * G + G - 1 + 1 + 2 + 1 + 2 * (far - 1)
+    n_local = G + 2 + len(args) - 6
     scratch = scratch + [
         pltpu.VMEM((nb, rows, d.block), BF16),
         pltpu.VMEM((near, far, rows, d.block), BF16),
@@ -579,9 +669,14 @@
         pltpu.VMEM((G * d.gw, d.out_cols), BF16),
         pltpu.VMEM((n_kv * rows, d.out_cols), F32),
         pltpu.VMEM((n_kv, rows, d.out_cols), BF16),
-        pltpu.VMEM((d.n_tp, per, rows, d.out_cols), BF16),
-        dma((n_send,)), dma((G, near)), dma((far,)), dma((near,)), dma((d.n_tp,)),
-        dma((G, far)), dma((G, near)), dma((G, n_kv)), dma((d.n_tp, per)), dma((n_local,)),
+        pltpu.VMEM((n_kv, rows, d.out_cols), BF16),
+        pltpu.VMEM((far, d.gw, d.out_cols), BF16),
+        pltpu.VMEM((near, rows, d.gw), BF16),
+        pltpu.VMEM((d.n_tp * near, per // near, rows, d.out_cols), BF16),
+        pltpu.VMEM((d.n_tp * near, per // near, rows, d.out_cols), BF16),
+        dma((n_send,)), dma((G,)), dma((far,)), dma((near, d.n_tp)), dma((d.n_tp,)),
+        dma((G,)), dma((G,)), dma((max(G - 1, 1),)), dma((max(G - 1, 1),)), dma((1,)),
+        dma((far,)), dma((1,)), dma((1,)), dma((n_local,)), dma((G,)),
     ]
     scratch = scratch + [pltpu.VMEM(item.shape, item.dtype) for item in args[6:]]
     past_v, past_b, past_c = (item.shape for item in args[-5:-2])

time: 54.8 us -> 51.1 us (0.932)
  Pallas kernels: 54 us -> 50.3 us
    pallas_call x1, Pallas kernels: 51.9 us -> 48.2 us  [mixer(): pl.pallas_call(functools.partial(mixer_kernel, d), out_shape=[pltpu.VMEM(...]
where the time goes in v3:
time: 51.1 us; the launch traced here: 50.9 us
  Pallas kernels  50.3 us (98%)
  between operations  0.65 us (1%)
    pallas_call x1, Pallas kernels, mixer(): pl.pallas_call(functools.partial(mixer_kernel, d), out_shape=[pltpu.VMEM(...  48.2 us
    pallas_call x1, Pallas kernels, store(): pl.pallas_call(functools.partial(store_kernel, count), out_shape=[jax.Sha...  2.1 us

profile of v3, /device:TPU:0, one launch (start us, length us, event | category | flops | bytes accessed | tf_op | source)
XLA Modules:
  0.0 50.9 jit_solution(5676853397384112695)
XLA Ops:
  0.6 48.2 %mixer.1 = (bf16[4,4,1024]{2,1,0:T(4,128)(2,1)S(1)}, f32[4,2048,128]{2,1,0:T(8,128)S(1)}, bf16[7,4,2048]{2,1,0:T(4,128)(2,1)S(1)}, bf16[7,4,512]{2,1,0:T(4,128)(...) custom-call(bf16[128,2048]{1,0:T(8,128)(2,1)} %refs_0_.1, bf16[128,2048]{1,0:T(8,128)(2,1)} %refs_1_.1, ...), custom_call_target="tpu_custom_call" | custom-call | tf_op jit(solution)/shard_map/mixer/pallas_call | solution.py:683
  48.8 2.1 %store.1 = (bf16[4,4,1024]{2,1,0:T(4,128)(2,1)}, f32[4,2048,128]{2,1,0:T(8,128)}, bf16[7,4,2048]{2,1,0:T(4,128)(2,1)}, bf16[7,4,512]{2,1,0:T(4,128)(2,1)}, bf16[...) custom-call(bf16[4,4,1024]{2,1,0:T(4,128)(2,1)S(1)} %get-tuple-element.18.refs_0_, ...), custom_call_target="tpu_custom_call" | custom-call | tf_op jit(solution)/shard_map/store/pallas_call | solution.py:716

commit v4 on v3

--- a/solution.py
+++ b/solution.py
@@ -396,6 +396,57 @@
     step_now = (joined[:, 0 : d.heads] * scale[:, 0 : d.heads]).astype(BF16)
     put_seq(next_s, slice(None), step_now)
 
+    def weights(g):
+        mark(f'w_wait{g}')
+        wbuf[g][l] = stage[g][l]
+        arrive(first(wbuf[g], near - 1), w_sem.at[g])
+        mark(f'matmul{g}')
+        return wbuf[g][...].reshape(d.block, d.cols(g))
+
+    def product(g, left, weight):
+        return jnp.dot(left, weight, preferred_element_type=F32).astype(BF16)
+
+    via_z = {}
+
+    def early():
+        result = product(0, xs[l].reshape(far * rows, d.block), weights(0))
+        for z in range(far):
+            zmine[0][z, l] = result[z * rows : (z + 1) * rows]
+        via_z[0] = meter(zmine[0], far - 1)
+        for step in reversed(range(1, far)):
+            z = lax.rem(h + step, far)
+            src, dst = zmine[0].at[z, l], zin[0].at[h, l]
+            send(src, dst, z_sem.at[0], z * near + l, tp, via=via_z[0])
+
+    def project(g):
+        if g == 0:
+            mark('matmul0b')
+            places = [lax.rem(l + step, near) for step in range(1, near)]
+            left = jnp.concatenate(
+                [xs[k].reshape(far * rows, d.block) for k in places], axis=0
+            )
+            result = product(0, left, wbuf[0][...].reshape(d.block, d.cols(0)))
+            for i, k in enumerate(places):
+                for z in range(far):
+                    at = (i * far + z) * rows
+                    zmine[0][z, k] = result[at : at + rows]
+            for step in reversed(range(1, far)):
+                z = lax.rem(h + step, far)
+                for k in places:
+                    src, dst = zmine[0].at[z, k], zin[0].at[h, k]
+                    send(src, dst, z_sem.at[0], z * near + l, tp, via=via_z[0])
+            return
+        result = product(g, xs[...].reshape(n_kv * rows, d.block), weights(g))
+        for k in range(near):
+            for z in range(far):
+                at = (k * far + z) * rows
+                zmine[g][z, k] = result[at : at + rows]
+        via = meter(zmine[g], far - 1)
+        for step in reversed(range(1, far)):
+            z = lax.rem(h + step, far)
+            send(zmine[g].at[z], zin[g].at[h], z_sem.at[g], z * near + l, tp, via=via)
+
+    early()
     mark('tokp_wait')
     for step in range(1, near):
         k = lax.rem(l + near - step, near)
@@ -408,26 +459,6 @@
         for side in range(1, n_tp):
             t = lax.rem(tp + n_tp - side, n_tp)
             arrive(piece(k, t), xp_sem.at[k, t])
-
-    def project(g):
-        mark(f'w_wait{g}')
-        wbuf[g][l] = stage[g][l]
-        arrive(first(wbuf[g], near - 1), w_sem.at[g])
-        mark(f'matmul{g}')
-        cols = d.cols(g)
-        product = jnp.dot(
-            xs[...].reshape(n_kv * rows, d.block),
-            wbuf[g][...].reshape(d.block, cols),
-            preferred_element_type=F32,
-        ).astype(BF16)
-        for k in range(near):
-            for z in range(far):
-                at = (k * far + z) * rows
-                zmine[g][z, k] = product[at : at + rows]
-        via = meter(zmine[g], far - 1)
-        for step in reversed(range(1, far)):
-            z = lax.rem(h + step, far)
-            send(zmine[g].at[z], zin[g].at[h], z_sem.at[g], z * near + l, tp, via=via)
 
     def collect(g):
         mark(f'z_wait{g}')

time: 51.1 us -> 50.1 us (0.980)
  Pallas kernels: 50.3 us -> 49.3 us
    pallas_call x1, Pallas kernels: 48.2 us -> 47.2 us  [mixer(): pl.pallas_call(functools.partial(mixer_kernel, d), out_shape=[pltpu.VMEM(...]
where the time goes in v4:
time: 50.1 us; the launch traced here: 49.9 us
  Pallas kernels  49.3 us (98%)
  between operations  0.65 us (1%)
    pallas_call x1, Pallas kernels, mixer(): pl.pallas_call(functools.partial(mixer_kernel, d), out_shape=[pltpu.VMEM(...  47.2 us
    pallas_call x1, Pallas kernels, store(): pl.pallas_call(functools.partial(store_kernel, count), out_shape=[jax.Sha...  2.1 us

profile of v4, /device:TPU:0, one launch (start us, length us, event | category | flops | bytes accessed | tf_op | source)
XLA Modules:
  0.0 49.9 jit_solution(7850809535321388750)
XLA Ops:
  0.6 47.2 %mixer.1 = (bf16[4,4,1024]{2,1,0:T(4,128)(2,1)S(1)}, f32[4,2048,128]{2,1,0:T(8,128)S(1)}, bf16[7,4,2048]{2,1,0:T(4,128)(2,1)S(1)}, bf16[7,4,512]{2,1,0:T(4,128)(...) custom-call(bf16[128,2048]{1,0:T(8,128)(2,1)} %refs_0_.1, bf16[128,2048]{1,0:T(8,128)(2,1)} %refs_1_.1, ...), custom_call_target="tpu_custom_call" | custom-call | tf_op jit(solution)/shard_map/mixer/pallas_call | solution.py:714
  47.8 2.1 %store.1 = (bf16[4,4,1024]{2,1,0:T(4,128)(2,1)}, f32[4,2048,128]{2,1,0:T(8,128)}, bf16[7,4,2048]{2,1,0:T(4,128)(2,1)}, bf16[7,4,512]{2,1,0:T(4,128)(2,1)}, bf16[...) custom-call(bf16[4,4,1024]{2,1,0:T(4,128)(2,1)S(1)} %get-tuple-element.18.refs_0_, ...), custom_call_target="tpu_custom_call" | custom-call | tf_op jit(solution)/shard_map/store/pallas_call | solution.py:747

commit v5 on v4

--- a/solution.py
+++ b/solution.py
@@ -49,7 +49,7 @@
         return self.gw // self.near
 
     def thin(self, g):
-        return g * self.near < 2 * self.groups
+        return 2 * g % self.near == 0
 
     def cols(self, g):
         return 2 * self.part + (STATE_DIM if self.thin(g) else 0)
@@ -165,7 +165,7 @@
             stage_in(gate_w.at[:, lo : lo + part], stage[g].at[k, :, 0:part])
             stage_in(value_w.at[:, lo : lo + part], stage[g].at[k, :, part : 2 * part])
             if d.thin(g):
-                u = (g * near + k) % units
+                u = (2 * g + k) % units
                 source = (write_w, read_w)[u % 2]
                 stage_in(
                     source.at[:, u // 2 * N : (u // 2 + 1) * N],
@@ -491,7 +491,7 @@
 
         def unit(u):
             j, k = u // near, u % near
-            return rounded(back[j][k, :, 2 * part : 2 * part + N])
+            return rounded(back[j * near // 2][k, :, 2 * part : 2 * part + N])
 
         def window(past, now, out, cols):
             before = old(past, cols)
@@ -625,7 +625,7 @@
         (project, lambda g: 2.75 * g),
         (collect, lambda g: 8.0 + 3.0 * g if g else 5.6),
         (advance, lambda g: 12.0 + 2.7 * g if g else 9.0),
-        (forward, lambda g: 17.6 + 1.9 * g),
+        (forward, lambda g: 17.2 + 2.1 * g),
     )
     order_of = sorted(
         (when(g), i, g)

time: 50.1 us -> 49.5 us (0.988)
  Pallas kernels: 49.3 us -> 48.3 us
    pallas_call x1, Pallas kernels: 47.2 us -> 46.2 us  [mixer(): pl.pallas_call(functools.partial(mixer_kernel, d), out_shape=[pltpu.VMEM(...]
where the time goes in v5:
time: 49.5 us; the launch traced here: 49 us
  Pallas kernels  48.3 us (98%)
  between operations  0.65 us (1%)
    pallas_call x1, Pallas kernels, mixer(): pl.pallas_call(functools.partial(mixer_kernel, d), out_shape=[pltpu.VMEM(...  46.2 us
    pallas_call x1, Pallas kernels, store(): pl.pallas_call(functools.partial(store_kernel, count), out_shape=[jax.Sha...  2.1 us

profile of v5, /device:TPU:0, one launch (start us, length us, event | category | flops | bytes accessed | tf_op | source)
XLA Modules:
  0.0 49.0 jit_solution(1924918974861357721)
XLA Ops:
  0.6 46.2 %mixer.1 = (bf16[4,4,1024]{2,1,0:T(4,128)(2,1)S(1)}, f32[4,2048,128]{2,1,0:T(8,128)S(1)}, bf16[7,4,2048]{2,1,0:T(4,128)(2,1)S(1)}, bf16[7,4,512]{2,1,0:T(4,128)(...) custom-call(bf16[128,2048]{1,0:T(8,128)(2,1)} %refs_0_.1, bf16[128,2048]{1,0:T(8,128)(2,1)} %refs_1_.1, ...), custom_call_target="tpu_custom_call" | custom-call | tf_op jit(solution)/shard_map/mixer/pallas_call | solution.py:714
  46.9 2.1 %store.1 = (bf16[4,4,1024]{2,1,0:T(4,128)(2,1)}, f32[4,2048,128]{2,1,0:T(8,128)}, bf16[7,4,2048]{2,1,0:T(4,128)(2,1)}, bf16[7,4,512]{2,1,0:T(4,128)(2,1)}, bf16[...) custom-call(bf16[4,4,1024]{2,1,0:T(4,128)(2,1)S(1)} %get-tuple-element.18.refs_0_, ...), custom_call_target="tpu_custom_call" | custom-call | tf_op jit(solution)/shard_map/store/pallas_call | solution.py:747

commit v6 on v5

--- a/solution.py
+++ b/solution.py
@@ -418,23 +418,26 @@
             src, dst = zmine[0].at[z, l], zin[0].at[h, l]
             send(src, dst, z_sem.at[0], z * near + l, tp, via=via_z[0])
 
+    def batch(t):
+        places = [lax.rem(l + step, near) for step in range(1, near)]
+        left = jnp.concatenate(
+            [xs[k, pl.ds(t * fq, fq)].reshape(fq * rows, d.block) for k in places], axis=0
+        )
+        result = product(0, left, wbuf[0][...].reshape(d.block, d.cols(0)))
+        for i, k in enumerate(places):
+            for q in range(fq):
+                at = (i * fq + q) * rows
+                zmine[0][t * fq + q, k] = result[at : at + rows]
+        for q in range(fq):
+            z = t * fq + q
+            for k in places:
+                src, dst = zmine[0].at[z, k], zin[0].at[h, k]
+                send(src, dst, z_sem.at[0], z * near + l, tp, z != h, via=via_z[0])
+
     def project(g):
         if g == 0:
-            mark('matmul0b')
-            places = [lax.rem(l + step, near) for step in range(1, near)]
-            left = jnp.concatenate(
-                [xs[k].reshape(far * rows, d.block) for k in places], axis=0
-            )
-            result = product(0, left, wbuf[0][...].reshape(d.block, d.cols(0)))
-            for i, k in enumerate(places):
-                for z in range(far):
-                    at = (i * far + z) * rows
-                    zmine[0][z, k] = result[at : at + rows]
-            for step in reversed(range(1, far)):
-                z = lax.rem(h + step, far)
-                for k in places:
-                    src, dst = zmine[0].at[z, k], zin[0].at[h, k]
-                    send(src, dst, z_sem.at[0], z * near + l, tp, via=via_z[0])
+            for side in range(1, n_tp):
+                batch(lax.rem(tp + side, n_tp))
             return
         result = product(g, xs[...].reshape(n_kv * rows, d.block), weights(g))
         for k in range(near):
@@ -454,6 +457,7 @@
         for side in range(1, n_tp):
             t = lax.rem(tp + side, n_tp)
             send(piece(k, tp), piece(k, tp), xp_sem.at[k, tp], me, t, via=via_x)
+    batch(tp)
     for step in range(1, near):
         k = lax.rem(l + near - step, near)
         for side in range(1, n_tp):

time: 49.5 us -> 49.3 us (level)
  no operation moved by 1% of the time
where the time goes in v6:
time: 49.3 us; the launch traced here: 48.8 us
  Pallas kernels  48.1 us (98%)
  between operations  0.65 us (1%)
    pallas_call x1, Pallas kernels, mixer(): pl.pallas_call(functools.partial(mixer_kernel, d), out_shape=[pltpu.VMEM(...  46 us
    pallas_call x1, Pallas kernels, store(): pl.pallas_call(functools.partial(store_kernel, count), out_shape=[jax.Sha...  2.1 us

profile of v6, /device:TPU:0, one launch (start us, length us, event | category | flops | bytes accessed | tf_op | source)
XLA Modules:
  0.0 48.8 jit_solution(11663960904393343405)
XLA Ops:
  0.6 46.0 %mixer.1 = (bf16[4,4,1024]{2,1,0:T(4,128)(2,1)S(1)}, f32[4,2048,128]{2,1,0:T(8,128)S(1)}, bf16[7,4,2048]{2,1,0:T(4,128)(2,1)S(1)}, bf16[7,4,512]{2,1,0:T(4,128)(...) custom-call(bf16[128,2048]{1,0:T(8,128)(2,1)} %refs_0_.1, bf16[128,2048]{1,0:T(8,128)(2,1)} %refs_1_.1, ...), custom_call_target="tpu_custom_call" | custom-call | tf_op jit(solution)/shard_map/mixer/pallas_call | solution.py:718
  46.7 2.1 %store.1 = (bf16[4,4,1024]{2,1,0:T(4,128)(2,1)}, f32[4,2048,128]{2,1,0:T(8,128)}, bf16[7,4,2048]{2,1,0:T(4,128)(2,1)}, bf16[7,4,512]{2,1,0:T(4,128)(2,1)}, bf16[...) custom-call(bf16[4,4,1024]{2,1,0:T(4,128)(2,1)S(1)} %get-tuple-element.18.refs_0_, ...), custom_call_target="tpu_custom_call" | custom-call | tf_op jit(solution)/shard_map/store/pallas_call | solution.py:751
